TPU v7x, 32 devices: a whole 2x2x4 slice. The times are simulated.
32 devices in a mesh: gr: 2 (over x), fs: 8 (over z, y), tp: 2 (over core).
Axes of the slice: x: 2, y: 2, z: 4, core: 2. Of those that a mesh axis runs over, the one named last changes fastest.
Arguments:
- tokens: bfloat16 [4096, 2048], P(('gr', 'fs')), may hold values from -6 to 6
- norm_gain: float32 [2048], P(('gr', 'fs')), may hold values from 0.1 to 1.9
- gate_train: float32 [8, 2048, 1024], P(None, ('gr', 'fs'), 'tp'), may hold values from -0.125 to 0.125
- up_train: float32 [8, 2048, 1024], P(None, ('gr', 'fs'), 'tp'), may hold values from -0.125 to 0.125
- down_train: float32 [8, 1024, 2048], P(None, 'tp', ('gr', 'fs')), may hold values from -0.1875 to 0.1875
- expert_ids: int32 [4096, 2], P(('gr', 'fs')), may hold values from 0 to 7, all different within a row; in each aligned block of 256 rows (0 to 255, 256 to 511, ...) at most 128 rows name the same one
- route_score: float32 [4096, 2], P(('gr', 'fs')), may hold values from 0.05 to 1
Outputs:
- gate_ready: bfloat16 [8, 2048, 1024], P('fs', None, 'tp')
- up_ready: bfloat16 [8, 2048, 1024], P('fs', None, 'tp')
- down_ready: bfloat16 [8, 1024, 2048], P('fs', 'tp')
- mixed: bfloat16 [4096, 2048], P(('gr', 'fs'), 'tp')
Inputs may be any that keep to these rules, and one draw needn't show every extreme that they name: `expert_ids`: each row names two different experts. Among the 256 rows of one device no expert is named more than 128 times, and in every draw some expert is named exactly 128 times by some device's rows.
All inputs are finite; a program needn't handle non-finite values.
Results may differ from a plain program's by a relative error of at most 0.015.
Values may be sent and summed in bfloat16 or wider, within the bound.
A program may use at most 64 MiB of HBM per device.

v0:
```python
import functools

import jax
import jax.numpy as jnp
from jax import lax
from jax.experimental import pallas as pl
from jax.experimental.pallas import tpu as pltpu
from jax.sharding import PartitionSpec as P

epsilon = 1e-06
MESH = pl.DeviceIdType.MESH


def remote(src, dst, send_sem, recv_sem, where):
    return pltpu.make_async_remote_copy(
        src_ref=src, dst_ref=dst, send_sem=send_sem, recv_sem=recv_sem, device_id=where, device_id_type=MESH
    )


def greet(sizes):
    barrier = pltpu.get_barrier_semaphore()
    count = 0
    for name, size in sizes.items():
        me = lax.axis_index(name)
        for k in range(1, size):
            pl.semaphore_signal(barrier, inc=1, device_id={name: lax.rem(me + k, size)}, device_id_type=MESH)
            count += 1
    pl.semaphore_wait(barrier, count)


def spread_kernel(sizes, local, direct_down, gate, up, down, rows, keys, gate_out, up_out, down_out, rows_out, keys_out,
                  w_send, w_recv, g_send, g_recv, up_send, low_send, y_send, x_recv, t_send, t_recv, k_send, k_recv, own_sem):
    n_gr, n_fs, n_tp = sizes["gr"], sizes["fs"], sizes["tp"]
    g, f, p = lax.axis_index("gr"), lax.axis_index("fs"), lax.axis_index("tp")
    inner = 2 if n_fs % 2 == 0 else 1
    lines = n_fs // inner
    z, y = f // inner, lax.rem(f, inner)
    depth = gate.shape[1]
    half = rows.shape[1] // n_tp
    cols = pl.ds(pl.multiple_of(p * half, half), half)
    sources, outs = (gate, up, down), (gate_out, up_out, down_out)

    def place(w, block):
        start = pl.multiple_of(block * depth, depth)
        if w < 2:
            return outs[w].at[:, pl.ds(start, depth), :]
        return outs[w].at[:, :, pl.ds(start, depth)] if direct_down else outs[w].at[block]

    greet(sizes)

    own = [pltpu.make_async_copy(rows, rows_out.at[f], own_sem.at[0]),
           pltpu.make_async_copy(keys, keys_out.at[f], own_sem.at[1])]
    for w in range(3):
        own.append(pltpu.make_async_copy(sources[w].at[pl.ds(f * local, local)], place(w, g * n_fs + f), own_sem.at[2 + w]))

    def block_of(b):
        return rows_out.at[b, :, cols]

    def row_copy(b, first, kind, where):
        src = rows.at[:, cols] if first else block_of(b)
        return remote(src, block_of(b), {"u": up_send, "d": low_send, "y": y_send}[kind].at[b], x_recv.at[b], where)

    def tp_copy(b, j):
        return remote(block_of(b), block_of(b), t_send.at[j, b], t_recv.at[j, b], {"tp": lax.rem(p + j + 1, n_tp)})

    def go_up(b, first, act):
        @pl.when(z < lines - 1)
        def _():
            act(row_copy(b, first, "u", {"fs": lax.rem(f + inner, n_fs)}))

    def go_down(b, first, act):
        @pl.when(z > 0)
        def _():
            act(row_copy(b, first, "d", {"fs": lax.rem(f + n_fs - inner, n_fs)}))

    def go_side(b, first, act):
        if inner == 2:
            act(row_copy(b, first, "y", {"fs": f + 1 - 2 * y}))

    def start(c):
        c.start()

    def recv(c):
        c.wait_recv()

    def sent(c):
        c.wait_send()

    go_up(f, True, start)
    go_down(f, True, start)
    go_side(f, True, start)
    key_copies = []
    for k in range(1, n_fs):
        to = lax.rem(f + k, n_fs)
        c = remote(keys, keys_out.at[f], k_send.at[k], k_recv.at[k], {"fs": to})
        c.start()
        key_copies.append(c)
    for c in own:
        c.start()

    def gr_copy(w, b, k, j, first):
        src = sources[w].at[pl.ds(f * local, local)] if first else place(w, b)
        return remote(src, place(w, b), g_send.at[w, k, j], g_recv.at[w, k, j], {"gr": lax.rem(g + j + 1, n_gr)})

    for w in range(3):
        for j in range(n_gr - 1):
            gr_copy(w, g * n_fs + f, 0, j, True).start()

    for s in range(1, lines):
        @pl.when(z >= s)
        def _():
            b = f - s * inner
            row_copy(b, False, "u", {"fs": lax.rem(f + inner, n_fs)}).wait_recv()
            go_up(b, False, start)
            go_side(b, False, start)
            for j in range(n_tp - 1):
                tp_copy(b, j).start()

        @pl.when(z < lines - s)
        def _():
            b = f + s * inner
            row_copy(b, False, "d", {"fs": lax.rem(f + inner, n_fs)}).wait_recv()
            go_down(b, False, start)
            go_side(b, False, start)
            for j in range(n_tp - 1):
                tp_copy(b, j).start()

    def w_copy(w, k):
        to = lax.rem(f + k, n_fs)
        return remote(sources[w].at[pl.ds(to * local, local)], place(w, g * n_fs + f), w_send.at[w, k], w_recv.at[w, k], {"fs": to})

    for w in range(3):
        for k in range(1, n_fs):
            w_copy(w, k).start()

    if inner == 2:
        for s in range(lines):
            b = lax.rem(z + s, lines) * inner + 1 - y
            row_copy(b, False, "y", {"fs": f + 1 - 2 * y}).wait_recv()
            for j in range(n_tp - 1):
                tp_copy(b, j).start()

    for w in range(3):
        for k in range(1, n_fs):
            w_copy(w, k).wait_recv()
            b = g * n_fs + lax.rem(f + n_fs - k, n_fs)
            for j in range(n_gr - 1):
                gr_copy(w, b, k, j, False).start()

    for k in range(1, n_fs):
        b = lax.rem(f + k, n_fs)
        for j in range(n_tp - 1):
            c = tp_copy(b, j)
            c.wait_recv()
            c.wait_send()
    for c in key_copies:
        c.wait_recv()
        c.wait_send()
    for c in own:
        c.wait()
    go_up(f, True, sent)
    go_down(f, True, sent)
    go_side(f, True, sent)
    for s in range(1, lines):
        @pl.when(z >= s)
        def _():
            go_up(f - s * inner, False, sent)
            go_side(f - s * inner, False, sent)

        @pl.when(z < lines - s)
        def _():
            go_down(f + s * inner, False, sent)
            go_side(f + s * inner, False, sent)
    for w in range(3):
        for k in range(n_fs):
            if k:
                w_copy(w, k).wait_send()
            for j in range(n_gr - 1):
                c = gr_copy(w, g * n_fs + lax.rem(f + n_fs - k, n_fs), k, j, False)
                c.wait_recv()
                c.wait_send()


def return_kernel(sizes, part, out, held, total, t_send, t_recv, f_send, f_recv):
    n_fs, n_tp = sizes["fs"], sizes["tp"]
    f, p = lax.axis_index("fs"), lax.axis_index("tp")
    half = part.shape[2] // n_tp

    def cols(q):
        return pl.ds(pl.multiple_of(q * half, half), half)

    greet({"fs": n_fs, "tp": n_tp})
    order = list(range(1, n_fs)) + [0]

    def tp_copy(k, j):
        to = lax.rem(p + j + 1, n_tp)
        b = lax.rem(f + k, n_fs)
        return remote(part.at[b, :, cols(to)], held.at[j, b], t_send.at[j, k], t_recv.at[j, k], {"tp": to})

    def f_copy(k):
        b = lax.rem(f + k, n_fs)
        return remote(total.at[b], out.at[f], f_send.at[k], f_recv.at[k], {"fs": b})

    for k in order:
        for j in range(n_tp - 1):
            tp_copy(k, j).start()
    for k in order:
        b = lax.rem(f + k, n_fs)
        value = part[b, :, cols(p)].astype(jnp.float32)
        for j in range(n_tp - 1):
            tp_copy(k, j).wait_recv()
            value = value + held[j, b].astype(jnp.float32)
        value = value.astype(jnp.bfloat16)
        if k == 0:
            out[b] = value
        else:
            total[b] = value
            f_copy(k).start()
    for k in order:
        for j in range(n_tp - 1):
            tp_copy(k, j).wait_send()
        if k:
            f_copy(k).wait_recv()
            f_copy(k).wait_send()


def fused_kernel(sizes, gate, up, down, rows, keys, weight, gate_hbm, up_hbm, down_hbm, mixed,
                 gate_in, up_in, down_in, rows_in, keys_in, picked, hidden, part, held, total, back, acc,
                 w_send, w_recv, g_send, g_recv, up_send, low_send, y_send, x_recv, t_send, t_recv, k_send, k_recv,
                 p_send, p_recv, f_send, f_recv, own_sem, out_sem):
    n_gr, n_fs, n_tp = sizes["gr"], sizes["fs"], sizes["tp"]
    g, f, p = lax.axis_index("gr"), lax.axis_index("fs"), lax.axis_index("tp")
    inner = 2 if n_fs % 2 == 0 else 1
    lines = n_fs // inner
    z, y = f // inner, lax.rem(f, inner)
    depth = gate.shape[1]
    count, width = rows.shape
    slots = weight.shape[2]
    half = width // n_tp
    bf16, f32 = jnp.bfloat16, jnp.float32
    sources, outs, finals = (gate, up, down), (gate_in, up_in, down_in), (gate_hbm, up_hbm, down_hbm)

    def cols(q):
        return pl.ds(pl.multiple_of(q * half, half), half)

    def near(k):
        return lax.rem(f + k, n_fs)

    def place(w, block):
        span = pl.ds(pl.multiple_of(block * depth, depth), depth)
        return outs[w].at[span, :] if w < 2 else outs[w].at[:, span]

    above, below, beside = {"fs": near(inner)}, {"fs": near(n_fs - inner)}, {"fs": f + 1 - 2 * y}

    def block_of(b):
        return rows_in.at[b, :, cols(p)]

    def row_copy(b, first, sems, where):
        return remote(rows.at[:, cols(p)] if first else block_of(b), block_of(b), sems.at[b], x_recv.at[b], where)

    def tp_copy(b, j):
        return remote(block_of(b), block_of(b), t_send.at[j, b], t_recv.at[j, b], {"tp": lax.rem(p + j + 1, n_tp)})

    def go_up(b, first, act):
        @pl.when(z < lines - 1)
        def _():
            act(row_copy(b, first, up_send, above))

    def go_down(b, first, act):
        @pl.when(z > 0)
        def _():
            act(row_copy(b, first, low_send, below))

    def go_side(b, first, act):
        if inner == 2:
            act(row_copy(b, first, y_send, beside))

    def start(c):
        c.start()

    def sent(c):
        c.wait_send()

    def gr_copy(w, k, j):
        src = sources[w].at[f] if k == 0 else place(w, g * n_fs + near(n_fs - k))
        return remote(src, place(w, g * n_fs + near(n_fs - k)), g_send.at[w, k, j], g_recv.at[w, k, j],
                      {"gr": lax.rem(g + j + 1, n_gr)})

    def w_copy(w, k):
        to = near(k)
        return remote(sources[w].at[to], place(w, g * n_fs + f), w_send.at[w, k], w_recv.at[w, k], {"fs": to})

    def send_weights(w):
        for k in range(1, n_fs):
            w_copy(w, k).start()

    def pass_on(w, k):
        w_copy(w, k).wait_recv()
        for j in range(n_gr - 1):
            gr_copy(w, k, j).start()

    def line_step(s):
        @pl.when(z >= s)
        def _():
            b = f - s * inner
            row_copy(b, False, up_send, above).wait_recv()
            go_up(b, False, start)
            go_side(b, False, start)
            for j in range(n_tp - 1):
                tp_copy(b, j).start()

        @pl.when(z < lines - s)
        def _():
            b = f + s * inner
            row_copy(b, False, low_send, below).wait_recv()
            go_down(b, False, start)
            go_side(b, False, start)
            for j in range(n_tp - 1):
                tp_copy(b, j).start()

    def whole(w):
        for k in range(n_fs):
            for j in range(n_gr - 1):
                gr_copy(w, k, j).wait_recv()
        pltpu.make_async_copy(outs[w], finals[w].at[0], out_sem.at[w]).start()

    def pick_rows(b):
        table = keys_in[b]
        wanted = f * slots + lax.broadcasted_iota(jnp.int32, (slots, count), 0)
        hit = ((table[0:1, :] == wanted) | (table[1:2, :] == wanted)).astype(f32).astype(bf16)
        for c in range(0, width, 512):
            picked[pl.ds(pl.multiple_of(b * slots, slots), slots), c:c + 512] = jnp.dot(
                hit, rows_in[b, :, c:c + 512], preferred_element_type=f32).astype(bf16)

    greet(sizes)

    own = [pltpu.make_async_copy(rows, rows_in.at[f], own_sem.at[0]),
           pltpu.make_async_copy(keys, keys_in.at[f], own_sem.at[1])]
    for w in range(3):
        own.append(pltpu.make_async_copy(sources[w].at[f], place(w, g * n_fs + f), own_sem.at[2 + w]))

    def key_copy(k):
        return remote(keys, keys_in.at[f], k_send.at[k], k_recv.at[k], {"fs": near(k)})

    send_weights(0)
    go_up(f, True, start)
    go_down(f, True, start)
    go_side(f, True, start)
    for k in range(1, n_fs):
        key_copy(k).start()
    for c in own:
        c.start()
    for w in range(3):
        for j in range(n_gr - 1):
            gr_copy(w, 0, j).start()
    send_weights(1)
    for k in range(1, n_fs):
        pass_on(0, k)
    if lines > 1:
        line_step(1)
    for k in range(1, n_fs):
        pass_on(1, k)
    if lines > 2:
        line_step(2)
    send_weights(2)
    for s in range(3, lines):
        line_step(s)
    if inner == 2:
        for s in range(lines):
            b = lax.rem(z + s, lines) * inner + 1 - y
            row_copy(b, False, y_send, beside).wait_recv()
            for j in range(n_tp - 1):
                tp_copy(b, j).start()
    for c in own:
        c.wait()
    pick_rows(f)
    for k in range(1, n_fs):
        b = near(n_fs - k)
        for j in range(n_tp - 1):
            tp_copy(b, j).wait_recv()
        key_copy(k).wait_recv()
        pick_rows(b)
    whole(0)
    whole(1)
    group = 2 if n_fs % 2 == 0 else 1
    for i in range(n_fs // group):
        for k in range(1 + i * group, min(1 + (i + 1) * group, n_fs)):
            pass_on(2, k)
        span = slice(i * group * slots, (i + 1) * group * slots)
        gate_act = jnp.dot(picked[span, :], gate_in[...], preferred_element_type=f32)
        up_act = jnp.dot(picked[span, :], up_in[...], preferred_element_type=f32)
        hidden[span, :] = (gate_act / (1.0 + jnp.exp(-gate_act)) * up_act).astype(bf16)
    whole(2)

    order = list(range(1, n_fs)) + [0]

    def p_copy(k, j):
        to = lax.rem(p + j + 1, n_tp)
        b = near(k)
        return remote(part.at[b, :, cols(to)], held.at[j, b], p_send.at[j, k], p_recv.at[j, k], {"tp": to})

    def f_copy(k):
        return remote(total.at[near(k)], back.at[f], f_send.at[k], f_recv.at[k], {"fs": near(k)})

    for i in range(n_fs + 3):
        if i < n_fs:
            b = near(order[i])
            mine = hidden[pl.ds(pl.multiple_of(b * slots, slots), slots), :]
            for c in range(0, width, 512):
                part[b, :, c:c + 512] = jnp.dot(mine, down_in[:, c:c + 512], preferred_element_type=f32).astype(bf16)
        if 0 <= i - 1 < n_fs:
            for j in range(n_tp - 1):
                p_copy(order[i - 1], j).start()
        if 0 <= i - 2 < n_fs:
            k = order[i - 2]
            b = near(k)
            value = part[b, :, cols(p)].astype(f32)
            for j in range(n_tp - 1):
                p_copy(k, j).wait_recv()
                value = value + held[j, b].astype(f32)
            total[b] = value.astype(bf16)
        if 0 <= i - 3 < n_fs and order[i - 3]:
            f_copy(order[i - 3]).start()

    acc[...] = jnp.dot(weight[f], total[f], preferred_element_type=f32)
    for k in range(1, n_fs):
        f_copy(k).wait_recv()
        b = near(n_fs - k)
        acc[...] += jnp.dot(weight[b], back[b], preferred_element_type=f32)
    mixed[...] = acc[...].astype(bf16)

    for k in range(n_fs):
        for j in range(n_tp - 1):
            p_copy(k, j).wait_send()
        if k:
            f_copy(k).wait_send()
            key_copy(k).wait_send()
            for j in range(n_tp - 1):
                tp_copy(near(k), j).wait_send()
        for w in range(3):
            if k:
                w_copy(w, k).wait_send()
            for j in range(n_gr - 1):
                gr_copy(w, k, j).wait_send()
    go_up(f, True, sent)
    go_down(f, True, sent)
    go_side(f, True, sent)
    for s in range(1, lines):
        @pl.when(z >= s)
        def _():
            go_up(f - s * inner, False, sent)
            go_side(f - s * inner, False, sent)

        @pl.when(z < lines - s)
        def _():
            go_down(f + s * inner, False, sent)
            go_side(f + s * inner, False, sent)
    for w in range(3):
        pltpu.make_async_copy(outs[w], finals[w].at[0], out_sem.at[w]).wait()


def run_fused(sizes, gate_cast, up_cast, down_cast, normed, keys, weight):
    n_gr, n_fs, n_tp = sizes["gr"], sizes["fs"], sizes["tp"]
    _, depth, hid = gate_cast.shape
    count, width = normed.shape
    slots = weight.shape[2]
    half = width // n_tp
    bf16, dma = jnp.bfloat16, pltpu.SemaphoreType.DMA
    vmem = pl.BlockSpec(memory_space=pltpu.VMEM)
    return pl.pallas_call(
        functools.partial(fused_kernel, sizes),
        out_shape=(
            jax.ShapeDtypeStruct((1, n_gr * n_fs * depth, hid), bf16),
            jax.ShapeDtypeStruct((1, n_gr * n_fs * depth, hid), bf16),
            jax.ShapeDtypeStruct((1, hid, n_gr * n_fs * depth), bf16),
            jax.ShapeDtypeStruct((count, half), bf16),
        ),
        in_specs=[vmem] * 6,
        out_specs=[pl.BlockSpec(memory_space=pl.ANY)] * 3 + [vmem],
        scratch_shapes=[
            pltpu.VMEM((n_gr * n_fs * depth, hid), bf16), pltpu.VMEM((n_gr * n_fs * depth, hid), bf16),
            pltpu.VMEM((hid, n_gr * n_fs * depth), bf16),
            pltpu.VMEM((n_fs, count, width), bf16), pltpu.VMEM((n_fs, 8, count), jnp.int32),
            pltpu.VMEM((n_fs * slots, width), bf16), pltpu.VMEM((n_fs * slots, hid), bf16),
            pltpu.VMEM((n_fs, slots, width), bf16),
            pltpu.VMEM((max(n_tp - 1, 1), n_fs, slots, half), bf16),
            pltpu.VMEM((n_fs, slots, half), bf16), pltpu.VMEM((n_fs, slots, half), bf16),
            pltpu.VMEM((count, half), jnp.float32),
            dma((3, n_fs)), dma((3, n_fs)), dma((3, n_fs, n_gr)), dma((3, n_fs, n_gr)),
            dma((n_fs,)), dma((n_fs,)), dma((n_fs,)), dma((n_fs,)),
            dma((n_tp, n_fs)), dma((n_tp, n_fs)), dma((n_fs,)), dma((n_fs,)),
            dma((n_tp, n_fs)), dma((n_tp, n_fs)), dma((n_fs,)), dma((n_fs,)), dma((5,)), dma((3,)),
        ],
        compiler_params=pltpu.CompilerParams(collective_id=2, has_side_effects=True, vmem_limit_bytes=62 * 2**20),
        name="handover",
    )(gate_cast, up_cast, down_cast, normed, keys, weight)


def on_device(sizes, tokens, norm_gain, gate_train, up_train, down_train, expert_ids, route_score):
    n_gr, n_fs, n_tp = sizes["gr"], sizes["fs"], sizes["tp"]
    bf16 = jnp.bfloat16
    experts, depth, hid = gate_train.shape
    local = experts // n_fs
    count, width = tokens.shape
    capacity = 4 * count // experts
    gate_cast = (norm_gain[None, :, None] * gate_train).astype(bf16)
    up_cast = (norm_gain[None, :, None] * up_train).astype(bf16)
    down_cast = down_train.astype(bf16)
    floated = tokens.astype(jnp.float32)
    normed = (floated * lax.rsqrt(jnp.mean(floated * floated, axis=-1, keepdims=True) + epsilon)).astype(bf16)

    named = expert_ids[:, :, None] == jnp.arange(experts, dtype=jnp.int32)
    names = jnp.any(named, axis=1)
    earlier = jnp.arange(count)[:, None] > jnp.arange(count)[None, :]
    rank = jnp.dot(earlier.astype(bf16), names.astype(bf16), preferred_element_type=jnp.float32).astype(jnp.int32)
    slot = expert_ids * capacity + jnp.sum(jnp.where(named, rank[:, None, :], 0), axis=2)
    keys = jnp.concatenate([slot.T, jnp.full((6, count), -1, jnp.int32)], axis=0)

    share = route_score / jnp.sum(route_score, axis=-1, keepdims=True)
    direct_down = depth % 128 == 0
    if direct_down and local == 1 and capacity % 128 == 0:
        at = (jnp.arange(experts, dtype=jnp.int32)[:, None] * capacity + jnp.arange(capacity, dtype=jnp.int32))[:, None, :]
        weight = jnp.where(slot[None, :, :1] == at, share[None, :, :1], 0.0) + jnp.where(slot[None, :, 1:] == at, share[None, :, 1:], 0.0)
        return run_fused(sizes, gate_cast, up_cast, down_cast, normed, keys, weight.astype(bf16))

    down_shape = (local, hid, n_gr * n_fs * depth) if direct_down else (n_gr * n_fs, local, hid, depth)
    dma = pltpu.SemaphoreType.DMA
    gate_ready, up_ready, down_ready, gathered, all_keys = pl.pallas_call(
        functools.partial(spread_kernel, sizes, local, direct_down),
        out_shape=(
            jax.ShapeDtypeStruct((local, n_gr * n_fs * depth, hid), bf16),
            jax.ShapeDtypeStruct((local, n_gr * n_fs * depth, hid), bf16),
            jax.ShapeDtypeStruct(down_shape, bf16),
            jax.ShapeDtypeStruct((n_fs, count, width), bf16),
            jax.ShapeDtypeStruct((n_fs, 8, count), jnp.int32),
        ),
        in_specs=[pl.BlockSpec(memory_space=pltpu.VMEM)] * 5,
        out_specs=[pl.BlockSpec(memory_space=pl.ANY)] * 5,
        scratch_shapes=[
            dma((3, n_fs)), dma((3, n_fs)), dma((3, n_fs, n_gr)), dma((3, n_fs, n_gr)),
            dma((n_fs,)), dma((n_fs,)), dma((n_fs,)), dma((n_fs,)),
            dma((n_tp, n_fs)), dma((n_tp, n_fs)), dma((n_fs,)), dma((n_fs,)), dma((5,)),
        ],
        compiler_params=pltpu.CompilerParams(collective_id=0, has_side_effects=True),
        name="spread",
    )(gate_cast, up_cast, down_cast, normed, keys)
    if not direct_down:
        down_ready = down_ready.transpose(1, 2, 0, 3).reshape(local, hid, -1)

    wanted = (lax.axis_index("fs") * local * capacity + jnp.arange(local * capacity, dtype=jnp.int32))[None, :, None]
    pick = ((all_keys[:, 0][:, None, :] == wanted) | (all_keys[:, 1][:, None, :] == wanted)).astype(bf16)
    rows = jnp.einsum("sct,std->scd", pick, gathered, preferred_element_type=jnp.float32).astype(bf16)
    rows = rows.reshape(n_fs, local, capacity, width)
    gate_act = jnp.einsum("seck,ekh->sech", rows, gate_ready, preferred_element_type=jnp.float32)
    up_act = jnp.einsum("seck,ekh->sech", rows, up_ready, preferred_element_type=jnp.float32)
    hidden = (jax.nn.silu(gate_act) * up_act).astype(bf16)
    part = jnp.einsum("sech,ehk->seck", hidden, down_ready, preferred_element_type=jnp.float32).astype(bf16)
    part = part.reshape(n_fs, local * capacity, width)
    half = width // n_tp
    returned = pl.pallas_call(
        functools.partial(return_kernel, sizes),
        out_shape=jax.ShapeDtypeStruct((n_fs, local * capacity, half), bf16),
        in_specs=[pl.BlockSpec(memory_space=pltpu.VMEM)],
        out_specs=pl.BlockSpec(memory_space=pltpu.VMEM),
        scratch_shapes=[
            pltpu.VMEM((max(n_tp - 1, 1), n_fs, local * capacity, half), bf16),
            pltpu.VMEM((n_fs, local * capacity, half), bf16),
            dma((n_tp, n_fs)), dma((n_tp, n_fs)), dma((n_fs,)), dma((n_fs,)),
        ],
        compiler_params=pltpu.CompilerParams(collective_id=1, has_side_effects=True),
        name="giveback",
    )(part)
    at = jnp.arange(experts * capacity, dtype=jnp.int32)[None, :]
    weight = jnp.where(slot[:, :1] == at, share[:, :1], 0.0) + jnp.where(slot[:, 1:] == at, share[:, 1:], 0.0)
    mixed = jnp.dot(weight.astype(bf16), returned.reshape(experts * capacity, half), preferred_element_type=jnp.float32)
    return gate_ready, up_ready, down_ready, mixed.astype(bf16)


def solution(mesh):
    return jax.shard_map(
        functools.partial(on_device, dict(mesh.shape)),
        mesh=mesh,
        in_specs=(
            P(("gr", "fs"), None),
            P(("gr", "fs")),
            P(None, ("gr", "fs"), "tp"),
            P(None, ("gr", "fs"), "tp"),
            P(None, "tp", ("gr", "fs")),
            P(("gr", "fs"), None),
            P(("gr", "fs"), None),
        ),
        out_specs=(
            P("fs", None, "tp"),
            P("fs", None, "tp"),
            P("fs", "tp", None),
            P(("gr", "fs"), "tp"),
        ),
        check_vma=False,
    )
```

profile of v0, /device:TPU:0, one launch (start us, length us, event | category | flops | bytes accessed | tf_op | source)
XLA Modules:
  0.0 216.3 jit_solution(3164180798611766321)
XLA Ops:
  0.6 0.0 copy-start
  0.7 1.6 fusion
  2.3 0.7 reduce_sum.29
  3.0 0.7 broadcast_divide_fusion
  3.7 0.7 fusion.2
  4.3 0.1 iota_add_fusion
  4.4 0.2 convolution_convert_fusion
  4.6 0.7 select_reduce_fusion
  5.3 0.7 multiply_add_fusion
  6.0 0.6 concatenate.3.keys
  6.6 1.1 add_convert_fusion.weight
  7.7 0.0 copy-done
  7.7 0.0 copy-start.2
  7.7 1.2 fusion.1.rows
  8.9 0.0 copy-start.1
  8.9 0.0 copy-start.6
  8.9 2.9 %convert_element_type.25.down = bf16[8,512,128]{2,1,0:T(8,128)(2,1)} convert(f32[8,512,128]{2,1,0:T(8,128)} %param.11) | non-fusion elementwise | flops 524288 | bytes 3145728 | tf_op jit(solution)/shard_map/convert_element_type | solution.py:508
  11.8 0.0 copy-done.2
  11.8 0.0 copy-done.1
  11.8 0.0 copy-done.6
  11.8 2.0 multiply_convert_fusion
  13.8 194.7 %handover.1 = (bf16[1,2048,512]{2,1,0:T(8,128)(2,1)}, bf16[1,2048,512]{2,1,0:T(8,128)(2,1)}, bf16[1,512,2048]{2,1,0:T(8,128)(2,1)}, bf16[256,1024]{1,0:T(8,128)(2,1)}) custom-call(bf16[8,128,512]{2,1,0:T(8,128)(2,1)} %get-tuple-element.9.gate, bf16[8,128,512]{2,1,0:T(8,128)(2,1)} %get-tuple-element.8.up, bf16[8,512,128]{2,1,0:T(8,128)(2,1)} %convert_element_type.25.down, ...), custom_call_target="tpu_custom_call" | custom-call | tf_op jit(solution)/shard_map/handover/pallas_call | solution.py:470
  208.6 0.0 copy-start.4
  208.6 3.2 %copy.17 = bf16[1,2048,512]{2,1,0:T(8,128)(2,1)} copy(bf16[1,2048,512]{2,1,0:T(8,128)(2,1)} %get-tuple-element.14) | data formatting | bytes 4194304
  211.8 0.0 copy-done.4
  211.8 0.0 copy-start.3
  211.8 1.3 copy.18
  213.1 1.0 copy-done.3
  214.1 0.0 copy-start.5
  214.1 1.3 copy.19
  215.5 0.1 copy-done.5
  215.5 0.8 copy.20
  (4 shorter events, 0.0 us)
Async XLA Ops:
  0.6 7.0 %copy-start = (bf16[256,2048]{1,0:T(8,128)(2,1)S(1)}, bf16[256,2048]{1,0:T(8,128)(2,1)}, u32[]{:S(2)}) copy-start(bf16[256,2048]{1,0:T(8,128)(2,1)} %param.7) | copy-start | bytes 3145732
  7.7 4.1 %copy-start.2 = (f32[8,128,512]{2,1,0:T(8,128)S(1)}, f32[8,128,512]{2,1,0:T(8,128)}, u32[]{:S(2)}) copy-start(f32[8,128,512]{2,1,0:T(8,128)} %param.9) | copy-start | bytes 6291460
  8.9 2.9 %copy-start.1 = (f32[8,128,512]{2,1,0:T(8,128)S(1)}, f32[8,128,512]{2,1,0:T(8,128)}, u32[]{:S(2)}) copy-start(f32[8,128,512]{2,1,0:T(8,128)} %param.10) | copy-start | bytes 6291460
  8.9 2.9 %copy-start.6 = (f32[128]{0:T(128)S(1)}, f32[128]{0:T(128)}, u32[]{:S(2)}) copy-start(f32[128]{0:T(128)} %param.8) | copy-start | bytes 1540
  208.6 3.2 %copy-start.4 = (bf16[1,2048,512]{2,1,0:T(8,128)(2,1)S(1)}, bf16[1,2048,512]{2,1,0:T(8,128)(2,1)}, u32[]{:S(2)}) copy-start(bf16[1,2048,512]{2,1,0:T(8,128)(2,1)} %get-tuple-element.15) | copy-start | bytes 6291460
  211.8 2.3 %copy-start.3 = (bf16[1,512,2048]{2,1,0:T(8,128)(2,1)S(1)}, bf16[1,512,2048]{2,1,0:T(8,128)(2,1)}, u32[]{:S(2)}) copy-start(bf16[1,512,2048]{2,1,0:T(8,128)(2,1)} %get-tuple-element.16) | copy-start | bytes 6291460
  214.1 1.4 copy-start.5
where the time goes:
time: 217 us; the launch traced here: 216 us
  Pallas kernels  195 us (90%)
  other arithmetic  12.4 us (6%)
  local copies, waits for them, and re-layouts  8.36 us (4%)
    pallas_call x1, Pallas kernels, run_fused(): pl.pallas_call(functools.partial(fused_kernel, sizes), out_shape=(jax.Sha...  195 us
    unnamed x18, local copies, waits for them, and re-layouts  7.75 us

commit v1 on v0

--- a/solution.py
+++ b/solution.py
@@ -224,276 +224,371 @@
             f_copy(k).wait_send()
 
 
-def fused_kernel(sizes, gate, up, down, rows, keys, weight, gate_hbm, up_hbm, down_hbm, mixed,
-                 gate_in, up_in, down_in, rows_in, keys_in, picked, hidden, part, held, total, back, acc,
-                 w_send, w_recv, g_send, g_recv, up_send, low_send, y_send, x_recv, t_send, t_recv, k_send, k_recv,
-                 p_send, p_recv, f_send, f_recv, own_sem, out_sem):
-    n_gr, n_fs, n_tp = sizes["gr"], sizes["fs"], sizes["tp"]
+def handover_kernel(sizes, tokens, gain, ids, score, gate_hbm, up_hbm, down_hbm, gate_out, up_out, down_out, mixed,
+                    gate_raw, up_raw, down_raw, gate_cut, up_cut, down_cut, rows_in, meta, picked, hidden, part, held,
+                    total, back, collect, far_out, far_in, near_w, gate_w,
+                    load_sem, w_send, w_recv, g_send, g_recv, x_recv, line_send, y_send, t_send, t_recv, k_send, k_recv,
+                    p_send, p_recv, n_send, n_recv, c_send, c_recv, o_send, o_recv):
+    n_fs = sizes["fs"]
     g, f, p = lax.axis_index("gr"), lax.axis_index("fs"), lax.axis_index("tp")
-    inner = 2 if n_fs % 2 == 0 else 1
-    lines = n_fs // inner
-    z, y = f // inner, lax.rem(f, inner)
-    depth = gate.shape[1]
-    count, width = rows.shape
-    slots = weight.shape[2]
-    half = width // n_tp
+    z, y = f // 2, lax.rem(f, 2)
+    low, side = lax.rem(z, 2), z // 2
+    depth = gate_hbm.shape[1]
+    count, width = tokens.shape
+    slots = back.shape[0] * 2 // n_fs
+    half = width // 2
+    span = half // 2
+    quad = n_fs // 2
     bf16, f32 = jnp.bfloat16, jnp.float32
-    sources, outs, finals = (gate, up, down), (gate_in, up_in, down_in), (gate_hbm, up_hbm, down_hbm)
+    raws, cuts, outs = (gate_raw, up_raw, down_raw), (gate_cut, up_cut, down_cut), (gate_out, up_out, down_out)
+    hbms = (gate_hbm, up_hbm, down_hbm)
+    near = [(0, 1), (1, 0), (1, 1)]
+    far = [(2, 0), (3, 0), (2, 1), (3, 1)]
+    index = {t: i for i, t in enumerate(near + far + [(0, 0)])}
+    door = 1 + side
+    is_door = z == door
+
+    def level(s):
+        lo = 1 - low if s % 2 else low
+        hi = 1 - side if s // 2 else side
+        return hi * 2 + lo
+
+    def peer(t):
+        return level(t[0]) * 2 + (1 - y if t[1] else y)
 
     def cols(q):
         return pl.ds(pl.multiple_of(q * half, half), half)
 
-    def near(k):
-        return lax.rem(f + k, n_fs)
-
     def place(w, block):
-        span = pl.ds(pl.multiple_of(block * depth, depth), depth)
-        return outs[w].at[span, :] if w < 2 else outs[w].at[:, span]
-
-    above, below, beside = {"fs": near(inner)}, {"fs": near(n_fs - inner)}, {"fs": f + 1 - 2 * y}
+        at = pl.ds(pl.multiple_of(block * depth, depth), depth)
+        return outs[w].at[0, at, :] if w < 2 else outs[w].at[0, :, at]
+
+    def w_copy(w, t):
+        to = peer(t)
+        return remote(cuts[w].at[to], place(w, g * n_fs + f), w_send.at[w, index[t]], w_recv.at[w, index[t]], {"fs": to})
+
+    def g_copy(w, t):
+        b = g * n_fs + peer(t)
+        src = cuts[w].at[f] if t == (0, 0) else place(w, b)
+        return remote(src, place(w, b), g_send.at[w, index[t]], g_recv.at[w, index[t]], {"gr": 1 - g})
+
+    def send_weights(w):
+        for t in near + far:
+            w_copy(w, t).start()
+        g_copy(w, (0, 0)).start()
+
+    def pass_on(w, t):
+        w_copy(w, t).wait_recv()
+        g_copy(w, t).start()
 
     def block_of(b):
         return rows_in.at[b, :, cols(p)]
 
-    def row_copy(b, first, sems, where):
-        return remote(rows.at[:, cols(p)] if first else block_of(b), block_of(b), sems.at[b], x_recv.at[b], where)
-
-    def tp_copy(b, j):
-        return remote(block_of(b), block_of(b), t_send.at[j, b], t_recv.at[j, b], {"tp": lax.rem(p + j + 1, n_tp)})
-
-    def go_up(b, first, act):
-        @pl.when(z < lines - 1)
-        def _():
-            act(row_copy(b, first, up_send, above))
-
-    def go_down(b, first, act):
-        @pl.when(z > 0)
-        def _():
-            act(row_copy(b, first, low_send, below))
-
-    def go_side(b, first, act):
-        if inner == 2:
-            act(row_copy(b, first, y_send, beside))
-
-    def start(c):
-        c.start()
-
-    def sent(c):
-        c.wait_send()
-
-    def gr_copy(w, k, j):
-        src = sources[w].at[f] if k == 0 else place(w, g * n_fs + near(n_fs - k))
-        return remote(src, place(w, g * n_fs + near(n_fs - k)), g_send.at[w, k, j], g_recv.at[w, k, j],
-                      {"gr": lax.rem(g + j + 1, n_gr)})
-
-    def w_copy(w, k):
-        to = near(k)
-        return remote(sources[w].at[to], place(w, g * n_fs + f), w_send.at[w, k], w_recv.at[w, k], {"fs": to})
-
-    def send_weights(w):
-        for k in range(1, n_fs):
-            w_copy(w, k).start()
-
-    def pass_on(w, k):
-        w_copy(w, k).wait_recv()
-        for j in range(n_gr - 1):
-            gr_copy(w, k, j).start()
-
-    def line_step(s):
-        @pl.when(z >= s)
-        def _():
-            b = f - s * inner
-            row_copy(b, False, up_send, above).wait_recv()
-            go_up(b, False, start)
-            go_side(b, False, start)
-            for j in range(n_tp - 1):
-                tp_copy(b, j).start()
-
-        @pl.when(z < lines - s)
-        def _():
-            b = f + s * inner
-            row_copy(b, False, low_send, below).wait_recv()
-            go_down(b, False, start)
-            go_side(b, False, start)
-            for j in range(n_tp - 1):
-                tp_copy(b, j).start()
-
-    def whole(w):
-        for k in range(n_fs):
-            for j in range(n_gr - 1):
-                gr_copy(w, k, j).wait_recv()
-        pltpu.make_async_copy(outs[w], finals[w].at[0], out_sem.at[w]).start()
+    def line_copy(b, i, to):
+        return remote(block_of(b), block_of(b), line_send.at[i], x_recv.at[b], {"fs": to})
+
+    def y_copy(b):
+        return remote(block_of(b), block_of(b), y_send.at[lax.div(b, 2)], x_recv.at[b], {"fs": z * 2 + 1 - y})
+
+    def tp_copy(b):
+        return remote(block_of(b), block_of(b), t_send.at[b], t_recv.at[b], {"tp": 1 - p})
+
+    def key_copy(t):
+        return remote(meta.at[f], meta.at[f], k_send.at[index[t]], k_recv.at[index[t]], {"fs": peer(t)})
+
+    def arrived(b):
+        line_copy(b, 0, z * 2 + 1 - y).wait_recv()
+
+    def cut(w):
+        pltpu.make_async_copy(hbms[w], raws[w], load_sem.at[w]).wait()
+        if w < 2:
+            scale = jnp.broadcast_to(gain[...], (128, depth)).T
+            for e in range(n_fs):
+                for c in range(0, raws[w].shape[2], 128):
+                    cuts[w][e, :, c:c + 128] = (scale * raws[w][e, :, c:c + 128]).astype(bf16)
+            outs[w][0, pl.ds(pl.multiple_of((g * n_fs + f) * depth, depth), depth), :] = cuts[w][f]
+        else:
+            for e in range(n_fs):
+                cuts[w][e] = raws[w][e].astype(bf16)
+            outs[w][0, :, pl.ds(pl.multiple_of((g * n_fs + f) * depth, depth), depth)] = cuts[w][f]
 
     def pick_rows(b):
-        table = keys_in[b]
-        wanted = f * slots + lax.broadcasted_iota(jnp.int32, (slots, count), 0)
-        hit = ((table[0:1, :] == wanted) | (table[1:2, :] == wanted)).astype(f32).astype(bf16)
+        wanted = (f * slots + lax.broadcasted_iota(jnp.int32, (slots, count), 0)).astype(f32)
+        hit = ((meta[b, 0:1, :] == wanted) | (meta[b, 1:2, :] == wanted)).astype(f32).astype(bf16)
         for c in range(0, width, 512):
             picked[pl.ds(pl.multiple_of(b * slots, slots), slots), c:c + 512] = jnp.dot(
                 hit, rows_in[b, :, c:c + 512], preferred_element_type=f32).astype(bf16)
 
-    greet(sizes)
-
-    own = [pltpu.make_async_copy(rows, rows_in.at[f], own_sem.at[0]),
-           pltpu.make_async_copy(keys, keys_in.at[f], own_sem.at[1])]
+    def shares(b):
+        wanted = (side * (quad * slots) + lax.broadcasted_iota(jnp.int32, (quad * slots, count), 0)).astype(f32)
+        table = jnp.where(meta[b, 0:1, :] == wanted, meta[b, 2:3, :], 0.0) + jnp.where(
+            meta[b, 1:2, :] == wanted, meta[b, 3:4, :], 0.0)
+        return table.T.astype(bf16)
+
     for w in range(3):
-        own.append(pltpu.make_async_copy(sources[w].at[f], place(w, g * n_fs + f), own_sem.at[2 + w]))
-
-    def key_copy(k):
-        return remote(keys, keys_in.at[f], k_send.at[k], k_recv.at[k], {"fs": near(k)})
-
+        pltpu.make_async_copy(hbms[w], raws[w], load_sem.at[w]).start()
+    barrier = pltpu.get_barrier_semaphore()
+    heard = 0
+    for name, size in sizes.items():
+        me = lax.axis_index(name)
+        for k in range(1, size):
+            pl.semaphore_signal(barrier, inc=1, device_id={name: lax.rem(me + k, size)}, device_id_type=MESH)
+            heard += 1
+
+    expert = lax.broadcasted_iota(jnp.int32, (16, count), 0)
+    names = ((ids[0:1, :] == expert) | (ids[1:2, :] == expert)).astype(f32).astype(bf16)
+    earlier = lax.broadcasted_iota(jnp.int32, (count, count), 0) < lax.broadcasted_iota(jnp.int32, (count, count), 1)
+    rank = jnp.dot(names, earlier.astype(f32).astype(bf16), preferred_element_type=f32) + (expert * slots).astype(f32)
+    both = score[0:1, :] + score[1:2, :]
+    table = [jnp.sum(jnp.where(ids[k:k + 1, :] == expert, rank, 0.0), axis=0, keepdims=True) for k in range(2)]
+    table += [score[k:k + 1, :] / both for k in range(2)]
+    for i in range(4):
+        meta[f, i:i + 1, :] = table[i]
+    meta[f, 4:8, :] = jnp.zeros((4, count), f32)
+
+    cut(0)
+    pl.semaphore_wait(barrier, heard)
     send_weights(0)
-    go_up(f, True, start)
-    go_down(f, True, start)
-    go_side(f, True, start)
-    for k in range(1, n_fs):
-        key_copy(k).start()
-    for c in own:
-        c.start()
+    for r in range(0, count, 32):
+        x = tokens[r:r + 32, :].astype(f32)
+        rows_in[f, r:r + 32, :] = (x * lax.rsqrt(jnp.mean(x * x, axis=-1, keepdims=True) + epsilon)).astype(bf16)
+    for t in near + far:
+        key_copy(t).start()
+    line_copy(f, 0, level(1) * 2 + y).start()
+    line_copy(f, 1, (2 - side) * 2 + y).start()
+    y_copy(f).start()
+    cut(1)
+    send_weights(1)
+    cut(2)
+
+    for w in range(2):
+        for t in near:
+            pass_on(w, t)
+    b = peer((1, 0))
+    arrived(b)
+    y_copy(b).start()
+    tp_copy(b).start()
+    for t in far:
+        pass_on(0, t)
+    for i, t in enumerate([(2, 0), (3, 0)]):
+        b = peer(t)
+        arrived(b)
+
+        @pl.when(is_door)
+        def _():
+            line_copy(b, 2 + i, level(1) * 2 + y).start()
+
+        y_copy(b).start()
+        tp_copy(b).start()
+    send_weights(2)
+    for t in [(0, 1), (1, 1), (2, 1), (3, 1)]:
+        b = peer(t)
+        arrived(b)
+        tp_copy(b).start()
+    pick_rows(f)
+    near_w[...] = shares(f)
+    for t in near + far:
+        key_copy(t).wait_recv()
+    for i in range(2):
+        gate_w[i] = shares(((1 - side) * 2 + i) * 2 + y)
+    for t in far:
+        pass_on(1, t)
+    for t in near + far:
+        tp_copy(peer(t)).wait_recv()
+        pick_rows(peer(t))
+    for w in range(2):
+        for t in near + far + [(0, 0)]:
+            g_copy(w, t).wait_recv()
+
+    def pair(s):
+        return pl.ds(pl.multiple_of(level(s) * (2 * slots), 2 * slots), 2 * slots)
+
+    order = [2, 3, 1, 0]
+    for i, s in enumerate(order):
+        gate_act = jnp.dot(picked[pair(s), :], gate_out[0], preferred_element_type=f32)
+        up_act = jnp.dot(picked[pair(s), :], up_out[0], preferred_element_type=f32)
+        hidden[pair(s), :] = (gate_act / (1.0 + jnp.exp(-gate_act)) * up_act).astype(bf16)
+        if i < len(near):
+            pass_on(2, near[i])
+
+    def seat(b):
+        return pl.ds(pl.multiple_of(b * slots, slots), slots)
+
+    mine = lax.rem(f, quad)
+
+    def stage(st, between):
+        at = side if st == 0 else 1 - side
+        here = pl.ds(pl.multiple_of(at * span, span), span)
+
+        def wide(q):
+            return pl.ds(pl.multiple_of(q * half + at * span, span), span)
+
+        def p_copy(s):
+            return remote(part.at[pair(s), wide(1 - p)], held.at[pair(s), here], p_send.at[st, s], p_recv.at[st, s], {"tp": 1 - p})
+
+        def n_copy(t):
+            return remote(total.at[seat(peer(t)), here], back.at[seat(mine), here], n_send.at[st, index[t]],
+                          n_recv.at[st, index[t]], {"fs": peer(t)})
+
+        def c_copy(t):
+            to = door * 2 + (1 - y if t[1] else y)
+            return remote(total.at[seat(peer(t)), here], collect.at[lax.rem(level(t[0]), 2), seat(mine), here],
+                          c_send.at[st, index[t]], c_recv.at[st, lax.rem(level(t[0]), 2), mine], {"fs": to})
+
+        def o_copy(i):
+            to = ((1 - side) * 2 + i) * 2 + y
+            return remote(far_out.at[i, :, here], far_in.at[:, here], o_send.at[st, i], o_recv.at[st], {"fs": to})
+
+        def compute(s):
+            for q in range(2):
+                part[pair(s), wide(q)] = jnp.dot(hidden[pair(s), :], down_out[0, :, wide(q)], preferred_element_type=f32).astype(bf16)
+
+        def add(s):
+            p_copy(s).wait_recv()
+            total[pair(s), here] = (part[pair(s), wide(p)].astype(f32) + held[pair(s), here].astype(f32)).astype(bf16)
+
+        def give(s):
+            for dy in range(2):
+                t = (s, dy)
+                if s > 1:
+                    if dy:
+                        c_copy(t).start()
+                    else:
+                        @pl.when(is_door)
+                        def _():
+                            collect[lax.rem(level(s), 2), seat(mine), here] = total[seat(peer(t)), here]
+
+                        @pl.when(z != door)
+                        def _():
+                            c_copy(t).start()
+                elif t == (0, 0):
+                    back[seat(mine), here] = total[seat(f), here]
+                else:
+                    n_copy(t).start()
+
+        for i in range(len(order) + 3):
+            if i < len(order):
+                compute(order[i])
+            if 0 <= i - 1 < len(order):
+                p_copy(order[i - 1]).start()
+            if 0 <= i - 2 < len(order):
+                add(order[i - 2])
+            if 0 <= i - 3 < len(order):
+                give(order[i - 3])
+            between(i)
+
+        @pl.when(is_door)
+        def _():
+            for i in range(2):
+                for k in range(1, quad):
+                    j = lax.rem(mine + k, quad)
+                    block = collect.at[i, seat(j), here]
+                    remote(block, block, c_send.at[st, 0], c_recv.at[st, i, j], {"tp": 1 - p}).wait_recv()
+                far_out[i, :, here] = jnp.dot(gate_w[i], collect[i, :, here], preferred_element_type=f32).astype(bf16)
+            for i in range(2):
+                o_copy(i).start()
+
+        def finish():
+            for t in near:
+                n_copy(t).wait_recv()
+
+        def finish_far():
+            there = pl.ds(pl.multiple_of((1 - at) * span, span), span)
+            block = far_in.at[:, there]
+            remote(block, block, o_send.at[st, 0], o_recv.at[st], {"tp": 1 - p}).wait_recv()
+
+        def drain():
+            for s in order:
+                p_copy(s).wait_send()
+            for t in near:
+                n_copy(t).wait_send()
+            for t in far:
+                if t[1]:
+                    c_copy(t).wait_send()
+                else:
+                    @pl.when(z != door)
+                    def _():
+                        c_copy(t).wait_send()
+
+            @pl.when(is_door)
+            def _():
+                for i in range(2):
+                    o_copy(i).wait_send()
+
+        return here, finish, finish_far, drain
+
+    for t in near + [(0, 0)]:
+        g_copy(2, t).wait_recv()
+    here, near_first, far_first, drain_first = stage(0, lambda i: None)
+    for t in far:
+        pass_on(2, t)
+    for t in far:
+        g_copy(2, t).wait_recv()
+    there, near_last, far_last, drain_last = stage(1, lambda i: None)
+    near_first()
+    acc = jnp.dot(near_w[...], back[:, here], preferred_element_type=f32)
+    near_last()
+    more = jnp.dot(near_w[...], back[:, there], preferred_element_type=f32)
+    far_first()
+    mixed[:, there] = (more + far_in[:, there].astype(f32)).astype(bf16)
+    far_last()
+    mixed[:, here] = (acc + far_in[:, here].astype(f32)).astype(bf16)
+
+    drain_first()
+    drain_last()
+    for t in near + far:
+        key_copy(t).wait_send()
+        tp_copy(peer(t)).wait_send()
     for w in range(3):
-        for j in range(n_gr - 1):
-            gr_copy(w, 0, j).start()
-    send_weights(1)
-    for k in range(1, n_fs):
-        pass_on(0, k)
-    if lines > 1:
-        line_step(1)
-    for k in range(1, n_fs):
-        pass_on(1, k)
-    if lines > 2:
-        line_step(2)
-    send_weights(2)
-    for s in range(3, lines):
-        line_step(s)
-    if inner == 2:
-        for s in range(lines):
-            b = lax.rem(z + s, lines) * inner + 1 - y
-            row_copy(b, False, y_send, beside).wait_recv()
-            for j in range(n_tp - 1):
-                tp_copy(b, j).start()
-    for c in own:
-        c.wait()
-    pick_rows(f)
-    for k in range(1, n_fs):
-        b = near(n_fs - k)
-        for j in range(n_tp - 1):
-            tp_copy(b, j).wait_recv()
-        key_copy(k).wait_recv()
-        pick_rows(b)
-    whole(0)
-    whole(1)
-    group = 2 if n_fs % 2 == 0 else 1
-    for i in range(n_fs // group):
-        for k in range(1 + i * group, min(1 + (i + 1) * group, n_fs)):
-            pass_on(2, k)
-        span = slice(i * group * slots, (i + 1) * group * slots)
-        gate_act = jnp.dot(picked[span, :], gate_in[...], preferred_element_type=f32)
-        up_act = jnp.dot(picked[span, :], up_in[...], preferred_element_type=f32)
-        hidden[span, :] = (gate_act / (1.0 + jnp.exp(-gate_act)) * up_act).astype(bf16)
-    whole(2)
-
-    order = list(range(1, n_fs)) + [0]
-
-    def p_copy(k, j):
-        to = lax.rem(p + j + 1, n_tp)
-        b = near(k)
-        return remote(part.at[b, :, cols(to)], held.at[j, b], p_send.at[j, k], p_recv.at[j, k], {"tp": to})
-
-    def f_copy(k):
-        return remote(total.at[near(k)], back.at[f], f_send.at[k], f_recv.at[k], {"fs": near(k)})
-
-    for i in range(n_fs + 3):
-        if i < n_fs:
-            b = near(order[i])
-            mine = hidden[pl.ds(pl.multiple_of(b * slots, slots), slots), :]
-            for c in range(0, width, 512):
-                part[b, :, c:c + 512] = jnp.dot(mine, down_in[:, c:c + 512], preferred_element_type=f32).astype(bf16)
-        if 0 <= i - 1 < n_fs:
-            for j in range(n_tp - 1):
-                p_copy(order[i - 1], j).start()
-        if 0 <= i - 2 < n_fs:
-            k = order[i - 2]
-            b = near(k)
-            value = part[b, :, cols(p)].astype(f32)
-            for j in range(n_tp - 1):
-                p_copy(k, j).wait_recv()
-                value = value + held[j, b].astype(f32)
-            total[b] = value.astype(bf16)
-        if 0 <= i - 3 < n_fs and order[i - 3]:
-            f_copy(order[i - 3]).start()
-
-    acc[...] = jnp.dot(weight[f], total[f], preferred_element_type=f32)
-    for k in range(1, n_fs):
-        f_copy(k).wait_recv()
-        b = near(n_fs - k)
-        acc[...] += jnp.dot(weight[b], back[b], preferred_element_type=f32)
-    mixed[...] = acc[...].astype(bf16)
-
-    for k in range(n_fs):
-        for j in range(n_tp - 1):
-            p_copy(k, j).wait_send()
-        if k:
-            f_copy(k).wait_send()
-            key_copy(k).wait_send()
-            for j in range(n_tp - 1):
-                tp_copy(near(k), j).wait_send()
-        for w in range(3):
-            if k:
-                w_copy(w, k).wait_send()
-            for j in range(n_gr - 1):
-                gr_copy(w, k, j).wait_send()
-    go_up(f, True, sent)
-    go_down(f, True, sent)
-    go_side(f, True, sent)
-    for s in range(1, lines):
-        @pl.when(z >= s)
-        def _():
-            go_up(f - s * inner, False, sent)
-            go_side(f - s * inner, False, sent)
-
-        @pl.when(z < lines - s)
-        def _():
-            go_down(f + s * inner, False, sent)
-            go_side(f + s * inner, False, sent)
-    for w in range(3):
-        pltpu.make_async_copy(outs[w], finals[w].at[0], out_sem.at[w]).wait()
-
-
-def run_fused(sizes, gate_cast, up_cast, down_cast, normed, keys, weight):
+        for t in near + far:
+            w_copy(w, t).wait_send()
+        for t in near + far + [(0, 0)]:
+            g_copy(w, t).wait_send()
+    line_copy(f, 0, level(1) * 2 + y).wait_send()
+    line_copy(f, 1, (2 - side) * 2 + y).wait_send()
+    for t in [(0, 0), (1, 0), (2, 0), (3, 0)]:
+        y_copy(peer(t)).wait_send()
+
+    @pl.when(is_door)
+    def _():
+        for i, t in enumerate([(2, 0), (3, 0)]):
+            line_copy(peer(t), 2 + i, level(1) * 2 + y).wait_send()
+
+
+def run_handover(sizes, slots, tokens, norm_gain, gate_train, up_train, down_train, expert_ids, route_score):
     n_gr, n_fs, n_tp = sizes["gr"], sizes["fs"], sizes["tp"]
-    _, depth, hid = gate_cast.shape
-    count, width = normed.shape
-    slots = weight.shape[2]
-    half = width // n_tp
-    bf16, dma = jnp.bfloat16, pltpu.SemaphoreType.DMA
-    vmem = pl.BlockSpec(memory_space=pltpu.VMEM)
+    _, depth, hid = gate_train.shape
+    count, width = tokens.shape
+    half, quad = width // n_tp, n_fs // 2
+    bf16, f32, dma = jnp.bfloat16, jnp.float32, pltpu.SemaphoreType.DMA
+    vmem, hbm = pl.BlockSpec(memory_space=pltpu.VMEM), pl.BlockSpec(memory_space=pl.ANY)
     return pl.pallas_call(
-        functools.partial(fused_kernel, sizes),
+        functools.partial(handover_kernel, sizes),
         out_shape=(
-            jax.ShapeDtypeStruct((1, n_gr * n_fs * depth, hid), bf16),
-            jax.ShapeDtypeStruct((1, n_gr * n_fs * depth, hid), bf16),
-            jax.ShapeDtypeStruct((1, hid, n_gr * n_fs * depth), bf16),
-            jax.ShapeDtypeStruct((count, half), bf16),
+            pltpu.VMEM((1, width, hid), bf16),
+            pltpu.VMEM((1, width, hid), bf16),
+            pltpu.VMEM((1, hid, width), bf16),
+            pltpu.VMEM((count, half), bf16),
         ),
-        in_specs=[vmem] * 6,
-        out_specs=[pl.BlockSpec(memory_space=pl.ANY)] * 3 + [vmem],
+        in_specs=[vmem] * 4 + [hbm] * 3,
+        out_specs=[vmem] * 4,
         scratch_shapes=[
-            pltpu.VMEM((n_gr * n_fs * depth, hid), bf16), pltpu.VMEM((n_gr * n_fs * depth, hid), bf16),
-            pltpu.VMEM((hid, n_gr * n_fs * depth), bf16),
-            pltpu.VMEM((n_fs, count, width), bf16), pltpu.VMEM((n_fs, 8, count), jnp.int32),
+            pltpu.VMEM((n_fs, depth, hid), f32), pltpu.VMEM((n_fs, depth, hid), f32), pltpu.VMEM((n_fs, hid, depth), f32),
+            pltpu.VMEM((n_fs, depth, hid), bf16), pltpu.VMEM((n_fs, depth, hid), bf16), pltpu.VMEM((n_fs, hid, depth), bf16),
+            pltpu.VMEM((n_fs, count, width), bf16), pltpu.VMEM((n_fs, 8, count), f32),
             pltpu.VMEM((n_fs * slots, width), bf16), pltpu.VMEM((n_fs * slots, hid), bf16),
-            pltpu.VMEM((n_fs, slots, width), bf16),
-            pltpu.VMEM((max(n_tp - 1, 1), n_fs, slots, half), bf16),
-            pltpu.VMEM((n_fs, slots, half), bf16), pltpu.VMEM((n_fs, slots, half), bf16),
-            pltpu.VMEM((count, half), jnp.float32),
-            dma((3, n_fs)), dma((3, n_fs)), dma((3, n_fs, n_gr)), dma((3, n_fs, n_gr)),
+            pltpu.VMEM((n_fs * slots, width), bf16), pltpu.VMEM((n_fs * slots, half), bf16),
+            pltpu.VMEM((n_fs * slots, half), bf16), pltpu.VMEM((quad * slots, half), bf16),
+            pltpu.VMEM((2, quad * slots, half), bf16), pltpu.VMEM((2, count, half), bf16), pltpu.VMEM((count, half), bf16),
+            pltpu.VMEM((count, quad * slots), bf16), pltpu.VMEM((2, count, quad * slots), bf16),
+            dma((3,)), dma((3, n_fs)), dma((3, n_fs)), dma((3, n_fs)), dma((3, n_fs)), dma((n_fs,)), dma((4,)), dma((n_fs,)),
             dma((n_fs,)), dma((n_fs,)), dma((n_fs,)), dma((n_fs,)),
-            dma((n_tp, n_fs)), dma((n_tp, n_fs)), dma((n_fs,)), dma((n_fs,)),
-            dma((n_tp, n_fs)), dma((n_tp, n_fs)), dma((n_fs,)), dma((n_fs,)), dma((5,)), dma((3,)),
+            dma((2, 4)), dma((2, 4)), dma((2, n_fs)), dma((2, n_fs)), dma((2, n_fs)), dma((2, 2, quad)),
+            dma((2, 2)), dma((2,)),
         ],
-        compiler_params=pltpu.CompilerParams(collective_id=2, has_side_effects=True, vmem_limit_bytes=62 * 2**20),
+        compiler_params=pltpu.CompilerParams(collective_id=2, has_side_effects=True, vmem_limit_bytes=54 * 2**20),
         name="handover",
-    )(gate_cast, up_cast, down_cast, normed, keys, weight)
+    )(tokens, norm_gain.reshape(1, depth), expert_ids.T, route_score.T, gate_train, up_train, down_train)
 
 
 def on_device(sizes, tokens, norm_gain, gate_train, up_train, down_train, expert_ids, route_score):
@@ -503,6 +598,10 @@
     local = experts // n_fs
     count, width = tokens.shape
     capacity = 4 * count // experts
+    direct_down = depth % 128 == 0
+    if direct_down and local == 1 and capacity % 128 == 0 and (n_gr, n_fs, n_tp) == (2, 8, 2):
+        return run_handover(sizes, capacity, tokens, norm_gain, gate_train, up_train, down_train, expert_ids, route_score)
+
     gate_cast = (norm_gain[None, :, None] * gate_train).astype(bf16)
     up_cast = (norm_gain[None, :, None] * up_train).astype(bf16)
     down_cast = down_train.astype(bf16)
@@ -517,12 +616,6 @@
     keys = jnp.concatenate([slot.T, jnp.full((6, count), -1, jnp.int32)], axis=0)
 
     share = route_score / jnp.sum(route_score, axis=-1, keepdims=True)
-    direct_down = depth % 128 == 0
-    if direct_down and local == 1 and capacity % 128 == 0:
-        at = (jnp.arange(experts, dtype=jnp.int32)[:, None] * capacity + jnp.arange(capacity, dtype=jnp.int32))[:, None, :]
-        weight = jnp.where(slot[None, :, :1] == at, share[None, :, :1], 0.0) + jnp.where(slot[None, :, 1:] == at, share[None, :, 1:], 0.0)
-        return run_fused(sizes, gate_cast, up_cast, down_cast, normed, keys, weight.astype(bf16))
-
     down_shape = (local, hid, n_gr * n_fs * depth) if direct_down else (n_gr * n_fs, local, hid, depth)
     dma = pltpu.SemaphoreType.DMA
     gate_ready, up_ready, down_ready, gathered, all_keys = pl.pallas_call(

time: 217 us -> 207 us (0.954)
  other arithmetic: 12.4 us -> 0 us
  Pallas kernels: 195 us -> 199 us
  local copies, waits for them, and re-layouts: 8.36 us -> 4.75 us
    convert_element_type x4 -> x0, other arithmetic: 7.22 us -> none  [the longest x1 2.88 us: on_device(): down_cast = down_train.astype(bf16)]
    pallas_call x1, Pallas kernels: 195 us -> 199 us  [run_handover(): pl.pallas_call(functools.partial(handover_kernel, sizes), out_shape=(pltp...]
    reduce_sum x3 -> x0, other arithmetic: 3.03 us -> none  [the longest x1 1.6 us: on_device(): jnp.mean(floated * floated, axis=-1, keepdims=True) + epsilon]
    unnamed x18 -> x4, local copies, waits for them, and re-layouts: 7.75 us -> 4.75 us
where the time goes in v1:
time: 207 us; the launch traced here: 205 us
  Pallas kernels  199 us (96%)
  local copies, waits for them, and re-layouts  4.75 us (2%)
    pallas_call x1, Pallas kernels, run_handover(): pl.pallas_call(functools.partial(handover_kernel, sizes), out_shape=(pltp...  199 us
    unnamed x4, local copies, waits for them, and re-layouts  4.75 us

profile of v1, /device:TPU:0, one launch (start us, length us, event | category | flops | bytes accessed | tf_op | source)
XLA Modules:
  0.0 204.7 jit_solution(1385035384560302026)
XLA Ops:
  0.6 199.3 %handover.1 = (bf16[1,2048,512]{2,1,0:T(8,128)(2,1)S(1)}, bf16[1,2048,512]{2,1,0:T(8,128)(2,1)S(1)}, bf16[1,512,2048]{2,1,0:T(8,128)(2,1)S(1)}, bf16[256,1024]{1,0:T(8,128)(2,1)S(1)}) custom-call(bf16[256,2048]{1,0:T(8,128)(2,1)} %tokens.1, f32[1,128]{1,0:T(1,128)} %bitcast.5, s32[2,256]{1,0:T(2,128)} %bitcast.3, f32[2,256]{1,0:T(2,128)} %bitcast.4, ...), custom_call_target="tpu_custom_call" | custom-call | tf_op jit(solution)/shard_map/handover/pallas_call | solution.py:565
  200.0 1.3 copy.15
  201.3 0.8 copy.18
  202.1 1.3 copy.16
  203.4 1.3 copy.17

commit v2 on v1

--- a/solution.py
+++ b/solution.py
@@ -225,14 +225,17 @@
 
 
 def handover_kernel(sizes, tokens, gain, ids, score, gate_hbm, up_hbm, down_hbm, gate_out, up_out, down_out, mixed,
-                    gate_raw, up_raw, down_raw, gate_cut, up_cut, down_cut, rows_in, meta, picked, hidden, part, held,
-                    total, back, collect, far_out, far_in, near_w, gate_w,
-                    load_sem, w_send, w_recv, g_send, g_recv, x_recv, line_send, y_send, t_send, t_recv, k_send, k_recv,
+                    gate_raw, up_raw, down_raw, gate_cut, up_cut, down_cut, rows_own, line_in, meta, y_pick, picked, hidden,
+                    part, held, total, back, collect, far_out, far_in, near_w, gate_w,
+                    load_sem, w_send, w_recv, g_send, g_recv, x_send, x_recv, y_send, y_recv, t_send, t_recv, k_send, k_recv,
                     p_send, p_recv, n_send, n_recv, c_send, c_recv, o_send, o_recv):
     n_fs = sizes["fs"]
     g, f, p = lax.axis_index("gr"), lax.axis_index("fs"), lax.axis_index("tp")
     z, y = f // 2, lax.rem(f, 2)
     low, side = lax.rem(z, 2), z // 2
+    door = 1 + side
+    is_door = z == door
+    role = 1 - (low + side - 2 * low * side)
     depth = gate_hbm.shape[1]
     count, width = tokens.shape
     slots = back.shape[0] * 2 // n_fs
@@ -243,21 +246,27 @@
     raws, cuts, outs = (gate_raw, up_raw, down_raw), (gate_cut, up_cut, down_cut), (gate_out, up_out, down_out)
     hbms = (gate_hbm, up_hbm, down_hbm)
     near = [(0, 1), (1, 0), (1, 1)]
-    far = [(2, 0), (3, 0), (2, 1), (3, 1)]
+    far = [(2, 0), (2, 1), (3, 0), (3, 1)]
     index = {t: i for i, t in enumerate(near + far + [(0, 0)])}
-    door = 1 + side
-    is_door = z == door
+    mine = lax.rem(f, quad)
 
     def level(s):
-        lo = 1 - low if s % 2 else low
-        hi = 1 - side if s // 2 else side
-        return hi * 2 + lo
+        return (z, z + 1 - 2 * low, 2 - side, 3 - 3 * side)[s]
 
     def peer(t):
         return level(t[0]) * 2 + (1 - y if t[1] else y)
 
+    def there(t):
+        return index[t] if t[0] < 2 else len(near) + 2 * role + t[1]
+
     def cols(q):
         return pl.ds(pl.multiple_of(q * half, half), half)
+
+    def seat(b):
+        return pl.ds(pl.multiple_of(b * slots, slots), slots)
+
+    def pair(s):
+        return pl.ds(pl.multiple_of(level(s) * (2 * slots), 2 * slots), 2 * slots)
 
     def place(w, block):
         at = pl.ds(pl.multiple_of(block * depth, depth), depth)
@@ -265,39 +274,47 @@
 
     def w_copy(w, t):
         to = peer(t)
-        return remote(cuts[w].at[to], place(w, g * n_fs + f), w_send.at[w, index[t]], w_recv.at[w, index[t]], {"fs": to})
+        return remote(cuts[w].at[to], place(w, g * n_fs + f), w_send.at[w, index[t]], w_recv.at[w, there(t)], {"fs": to})
+
+    def w_wait(w, t):
+        block = place(w, g * n_fs + peer(t))
+        remote(block, block, w_send.at[w, index[t]], w_recv.at[w, index[t]], {"fs": peer(t)}).wait_recv()
 
     def g_copy(w, t):
         b = g * n_fs + peer(t)
         src = cuts[w].at[f] if t == (0, 0) else place(w, b)
         return remote(src, place(w, b), g_send.at[w, index[t]], g_recv.at[w, index[t]], {"gr": 1 - g})
 
-    def send_weights(w):
-        for t in near + far:
-            w_copy(w, t).start()
-        g_copy(w, (0, 0)).start()
-
     def pass_on(w, t):
-        w_copy(w, t).wait_recv()
+        w_wait(w, t)
         g_copy(w, t).start()
 
-    def block_of(b):
-        return rows_in.at[b, :, cols(p)]
-
-    def line_copy(b, i, to):
-        return remote(block_of(b), block_of(b), line_send.at[i], x_recv.at[b], {"fs": to})
-
-    def y_copy(b):
-        return remote(block_of(b), block_of(b), y_send.at[lax.div(b, 2)], x_recv.at[b], {"fs": z * 2 + 1 - y})
-
-    def tp_copy(b):
-        return remote(block_of(b), block_of(b), t_send.at[b], t_recv.at[b], {"tp": 1 - p})
-
-    def key_copy(t):
-        return remote(meta.at[f], meta.at[f], k_send.at[index[t]], k_recv.at[index[t]], {"fs": peer(t)})
-
-    def arrived(b):
-        line_copy(b, 0, z * 2 + 1 - y).wait_recv()
+    def row_copy(s):
+        if s == 1:
+            return remote(rows_own.at[:, cols(p)], line_in.at[0], x_send.at[0], x_recv.at[0], {"fs": peer((1, 0))})
+        return remote(rows_own.at[:, cols(p)], line_in.at[1 + role], x_send.at[1], x_recv.at[1 + role], {"fs": peer((2, 0))})
+
+    def end_copy(s):
+        return remote(line_in.at[s - 1], line_in.at[s - 1], x_send.at[s], x_recv.at[s - 1], {"fs": peer((1, 0))})
+
+    def y_copy(s):
+        return remote(y_pick.at[s], picked.at[seat(peer((s, 0))), cols(p)], y_send.at[s], y_recv.at[s], {"fs": peer((0, 1))})
+
+    def y_wait(s):
+        block = picked.at[seat(peer((s, 1))), cols(p)]
+        remote(block, block, y_send.at[s], y_recv.at[s], {"fs": peer((0, 1))}).wait_recv()
+
+    def tp_copy(t):
+        block = picked.at[seat(peer(t)), cols(p)]
+        return remote(block, block, t_send.at[index[t]], t_recv.at[index[t]], {"tp": 1 - p})
+
+    def key_copy(s):
+        to = s if s < 2 else 2 + role
+        return remote(meta.at[f], meta.at[f], k_send.at[s], k_recv.at[to], {"fs": peer((s, 0))})
+
+    def key_wait(s):
+        block = meta.at[peer((s, 0))]
+        remote(block, block, k_send.at[s], k_recv.at[s], {"fs": peer((s, 0))}).wait_recv()
 
     def cut(w):
         pltpu.make_async_copy(hbms[w], raws[w], load_sem.at[w]).wait()
@@ -312,18 +329,28 @@
                 cuts[w][e] = raws[w][e].astype(bf16)
             outs[w][0, :, pl.ds(pl.multiple_of((g * n_fs + f) * depth, depth), depth)] = cuts[w][f]
 
-    def pick_rows(b):
-        wanted = (f * slots + lax.broadcasted_iota(jnp.int32, (slots, count), 0)).astype(f32)
+    def pick(b, expert, rows):
+        wanted = (expert * slots + lax.broadcasted_iota(jnp.int32, (slots, count), 0)).astype(f32)
         hit = ((meta[b, 0:1, :] == wanted) | (meta[b, 1:2, :] == wanted)).astype(f32).astype(bf16)
-        for c in range(0, width, 512):
-            picked[pl.ds(pl.multiple_of(b * slots, slots), slots), c:c + 512] = jnp.dot(
-                hit, rows_in[b, :, c:c + 512], preferred_element_type=f32).astype(bf16)
+        return jnp.dot(hit, rows, preferred_element_type=f32).astype(bf16)
 
     def shares(b):
         wanted = (side * (quad * slots) + lax.broadcasted_iota(jnp.int32, (quad * slots, count), 0)).astype(f32)
         table = jnp.where(meta[b, 0:1, :] == wanted, meta[b, 2:3, :], 0.0) + jnp.where(
             meta[b, 1:2, :] == wanted, meta[b, 3:4, :], 0.0)
         return table.T.astype(bf16)
+
+    def take_line(s, relay):
+        arriving = remote(line_in.at[s - 1], line_in.at[s - 1], x_send.at[0], x_recv.at[s - 1], {"fs": peer((1, 0))})
+        arriving.wait_recv()
+        if relay:
+            end_copy(s).start()
+        b = peer((s, 0))
+        key_wait(s)
+        y_pick[s] = pick(b, peer((0, 1)), line_in[s - 1])
+        picked[seat(b), cols(p)] = pick(b, f, line_in[s - 1])
+        y_copy(s).start()
+        tp_copy((s, 0)).start()
 
     for w in range(3):
         pltpu.make_async_copy(hbms[w], raws[w], load_sem.at[w]).start()
@@ -345,214 +372,267 @@
     for i in range(4):
         meta[f, i:i + 1, :] = table[i]
     meta[f, 4:8, :] = jnp.zeros((4, count), f32)
-
-    cut(0)
-    pl.semaphore_wait(barrier, heard)
-    send_weights(0)
     for r in range(0, count, 32):
         x = tokens[r:r + 32, :].astype(f32)
-        rows_in[f, r:r + 32, :] = (x * lax.rsqrt(jnp.mean(x * x, axis=-1, keepdims=True) + epsilon)).astype(bf16)
+        rows_own[r:r + 32, :] = (x * lax.rsqrt(jnp.mean(x * x, axis=-1, keepdims=True) + epsilon)).astype(bf16)
+    y_pick[0] = pick(f, peer((0, 1)), rows_own[:, cols(p)])
+    pl.semaphore_wait(barrier, heard)
+    for s in range(1, 4):
+        key_copy(s).start()
+    row_copy(1).start()
+    row_copy(2).start()
+    y_copy(0).start()
+    cut(0)
+    for t in near:
+        w_copy(0, t).start()
+    g_copy(0, (0, 0)).start()
+    cut(1)
+    for w, ts in [(1, near), (0, far), (1, far)]:
+        for t in ts:
+            w_copy(w, t).start()
+    g_copy(1, (0, 0)).start()
+    cut(2)
+    w_copy(2, (0, 1)).start()
+    g_copy(2, (0, 0)).start()
+
+    @pl.when(z != door)
+    def _():
+        w_copy(2, (1, 0)).start()
+        w_copy(2, (1, 1)).start()
+
+    for c in range(0, width, 512):
+        picked[seat(f), c:c + 512] = pick(f, f, rows_own[:, c:c + 512])
+    near_w[...] = shares(f)
+    y_wait(0)
+    tp_copy((0, 1)).start()
+    pass_on(0, (0, 1))
+    pass_on(1, (0, 1))
+    take_line(1, False)
+
+    @pl.when(is_door)
+    def _():
+        take_line(2, True)
+
+    pass_on(0, (1, 0))
+    pass_on(0, (1, 1))
+
+    @pl.when(is_door)
+    def _():
+        take_line(3, True)
+
+    pass_on(1, (1, 0))
+    pass_on(1, (1, 1))
+
+    @pl.when(is_door)
+    def _():
+        for i in range(2):
+            gate_w[i] = shares(peer((2 + i, 0)))
+
+    pass_on(0, (3, 0))
+    pass_on(0, (3, 1))
+    pass_on(0, (2, 0))
+    pass_on(0, (2, 1))
+    y_wait(1)
+    tp_copy((1, 1)).start()
+
+    @pl.when(z != door)
+    def _():
+        take_line(2, False)
+
+
+    @pl.when(is_door)
+    def _():
+        for s in (2, 3):
+            y_wait(s)
+            tp_copy((s, 1)).start()
+
+    pass_on(2, (0, 1))
+    pass_on(1, (3, 0))
+    pass_on(1, (3, 1))
+
+    @pl.when(z != door)
+    def _():
+        take_line(3, False)
+        y_wait(2)
+        tp_copy((2, 1)).start()
+
+    pass_on(1, (2, 0))
+    pass_on(1, (2, 1))
+
+    @pl.when(is_door)
+    def _():
+        w_copy(2, (1, 0)).start()
+        w_copy(2, (1, 1)).start()
+
+    for t in far:
+        w_copy(2, t).start()
+
+    @pl.when(z != door)
+    def _():
+        y_wait(3)
+        tp_copy((3, 1)).start()
+
+    for t in near[1:]:
+        pass_on(2, t)
     for t in near + far:
-        key_copy(t).start()
-    line_copy(f, 0, level(1) * 2 + y).start()
-    line_copy(f, 1, (2 - side) * 2 + y).start()
-    y_copy(f).start()
-    cut(1)
-    send_weights(1)
-    cut(2)
-
-    for w in range(2):
-        for t in near:
-            pass_on(w, t)
-    b = peer((1, 0))
-    arrived(b)
-    y_copy(b).start()
-    tp_copy(b).start()
-    for t in far:
-        pass_on(0, t)
-    for i, t in enumerate([(2, 0), (3, 0)]):
-        b = peer(t)
-        arrived(b)
-
-        @pl.when(is_door)
-        def _():
-            line_copy(b, 2 + i, level(1) * 2 + y).start()
-
-        y_copy(b).start()
-        tp_copy(b).start()
-    send_weights(2)
-    for t in [(0, 1), (1, 1), (2, 1), (3, 1)]:
-        b = peer(t)
-        arrived(b)
-        tp_copy(b).start()
-    pick_rows(f)
-    near_w[...] = shares(f)
-    for t in near + far:
-        key_copy(t).wait_recv()
-    for i in range(2):
-        gate_w[i] = shares(((1 - side) * 2 + i) * 2 + y)
-    for t in far:
-        pass_on(1, t)
-    for t in near + far:
-        tp_copy(peer(t)).wait_recv()
-        pick_rows(peer(t))
+        tp_copy(t).wait_recv()
     for w in range(2):
         for t in near + far + [(0, 0)]:
             g_copy(w, t).wait_recv()
-
-    def pair(s):
-        return pl.ds(pl.multiple_of(level(s) * (2 * slots), 2 * slots), 2 * slots)
-
     order = [2, 3, 1, 0]
-    for i, s in enumerate(order):
+
+    def act(s):
         gate_act = jnp.dot(picked[pair(s), :], gate_out[0], preferred_element_type=f32)
         up_act = jnp.dot(picked[pair(s), :], up_out[0], preferred_element_type=f32)
         hidden[pair(s), :] = (gate_act / (1.0 + jnp.exp(-gate_act)) * up_act).astype(bf16)
-        if i < len(near):
-            pass_on(2, near[i])
-
-    def seat(b):
-        return pl.ds(pl.multiple_of(b * slots, slots), slots)
-
-    mine = lax.rem(f, quad)
-
-    def stage(st, between):
-        at = side if st == 0 else 1 - side
-        here = pl.ds(pl.multiple_of(at * span, span), span)
-
-        def wide(q):
-            return pl.ds(pl.multiple_of(q * half + at * span, span), span)
-
-        def p_copy(s):
-            return remote(part.at[pair(s), wide(1 - p)], held.at[pair(s), here], p_send.at[st, s], p_recv.at[st, s], {"tp": 1 - p})
-
-        def n_copy(t):
-            return remote(total.at[seat(peer(t)), here], back.at[seat(mine), here], n_send.at[st, index[t]],
-                          n_recv.at[st, index[t]], {"fs": peer(t)})
-
-        def c_copy(t):
-            to = door * 2 + (1 - y if t[1] else y)
-            return remote(total.at[seat(peer(t)), here], collect.at[lax.rem(level(t[0]), 2), seat(mine), here],
-                          c_send.at[st, index[t]], c_recv.at[st, lax.rem(level(t[0]), 2), mine], {"fs": to})
-
-        def o_copy(i):
-            to = ((1 - side) * 2 + i) * 2 + y
-            return remote(far_out.at[i, :, here], far_in.at[:, here], o_send.at[st, i], o_recv.at[st], {"fs": to})
-
+
+    def here(st, base=0):
+        size = span if st == 0 else 2 * depth
+        return pl.ds(pl.multiple_of(base + (side * span if st == 0 else level(1 + st) * (2 * depth)), size), size)
+
+    def p_copy(st, s):
+        return remote(part.at[pair(s), here(st, (1 - p) * half)], held.at[pair(s), here(st)], p_send.at[st, s], p_recv.at[st, s],
+                      {"tp": 1 - p})
+
+    def n_copy(st, t):
+        return remote(total.at[seat(peer(t)), here(st)], back.at[seat(mine), here(st)], n_send.at[st, index[t]],
+                      n_recv.at[st, index[t]], {"fs": peer(t)})
+
+    def c_copy(st, t):
+        return remote(total.at[seat(peer(t)), here(st)], collect.at[t[0] - 2, seat(mine), here(st)], c_send.at[st, index[t]],
+                      c_recv.at[st, t[0] - 2, mine], {"fs": door * 2 + (1 - y if t[1] else y)})
+
+    def o_copy(st, i):
+        return remote(far_out.at[i, :, here(st)], far_in.at[:, here(st)], o_send.at[st, i], o_recv.at[st], {"fs": peer((2 + i, 0))})
+
+    def stage(st):
         def compute(s):
             for q in range(2):
-                part[pair(s), wide(q)] = jnp.dot(hidden[pair(s), :], down_out[0, :, wide(q)], preferred_element_type=f32).astype(bf16)
+                part[pair(s), here(st, q * half)] = jnp.dot(
+                    hidden[pair(s), :], down_out[0, :, here(st, q * half)], preferred_element_type=f32).astype(bf16)
 
         def add(s):
-            p_copy(s).wait_recv()
-            total[pair(s), here] = (part[pair(s), wide(p)].astype(f32) + held[pair(s), here].astype(f32)).astype(bf16)
+            p_copy(st, s).wait_recv()
+            total[pair(s), here(st)] = (part[pair(s), here(st, p * half)].astype(f32) + held[pair(s), here(st)].astype(f32)).astype(bf16)
 
         def give(s):
             for dy in range(2):
                 t = (s, dy)
-                if s > 1:
-                    if dy:
-                        c_copy(t).start()
-                    else:
-                        @pl.when(is_door)
-                        def _():
-                            collect[lax.rem(level(s), 2), seat(mine), here] = total[seat(peer(t)), here]
-
-                        @pl.when(z != door)
-                        def _():
-                            c_copy(t).start()
-                elif t == (0, 0):
-                    back[seat(mine), here] = total[seat(f), here]
+                if t == (0, 0):
+                    back[seat(mine), here(st)] = total[seat(f), here(st)]
+                elif s == 0:
+                    n_copy(st, t).start()
+                elif s == 1:
+                    pass
+                elif dy:
+                    c_copy(st, t).start()
                 else:
-                    n_copy(t).start()
+                    @pl.when(is_door)
+                    def _():
+                        collect[s - 2, seat(mine), here(st)] = total[seat(peer(t)), here(st)]
+
+                    @pl.when(z != door)
+                    def _():
+                        c_copy(st, t).start()
 
         for i in range(len(order) + 3):
             if i < len(order):
+                if st == 0:
+                    act(order[i])
                 compute(order[i])
             if 0 <= i - 1 < len(order):
-                p_copy(order[i - 1]).start()
+                p_copy(st, order[i - 1]).start()
             if 0 <= i - 2 < len(order):
                 add(order[i - 2])
             if 0 <= i - 3 < len(order):
                 give(order[i - 3])
-            between(i)
-
+
+    def merge(st):
         @pl.when(is_door)
         def _():
             for i in range(2):
                 for k in range(1, quad):
                     j = lax.rem(mine + k, quad)
-                    block = collect.at[i, seat(j), here]
+                    block = collect.at[i, seat(j), here(st)]
                     remote(block, block, c_send.at[st, 0], c_recv.at[st, i, j], {"tp": 1 - p}).wait_recv()
-                far_out[i, :, here] = jnp.dot(gate_w[i], collect[i, :, here], preferred_element_type=f32).astype(bf16)
-            for i in range(2):
-                o_copy(i).start()
-
-        def finish():
-            for t in near:
-                n_copy(t).wait_recv()
-
-        def finish_far():
-            there = pl.ds(pl.multiple_of((1 - at) * span, span), span)
-            block = far_in.at[:, there]
-            remote(block, block, o_send.at[st, 0], o_recv.at[st], {"tp": 1 - p}).wait_recv()
-
-        def drain():
-            for s in order:
-                p_copy(s).wait_send()
-            for t in near:
-                n_copy(t).wait_send()
-            for t in far:
-                if t[1]:
-                    c_copy(t).wait_send()
-                else:
-                    @pl.when(z != door)
-                    def _():
-                        c_copy(t).wait_send()
-
-            @pl.when(is_door)
-            def _():
-                for i in range(2):
-                    o_copy(i).wait_send()
-
-        return here, finish, finish_far, drain
+                far_out[i, :, here(st)] = jnp.dot(gate_w[i], collect[i, :, here(st)], preferred_element_type=f32).astype(bf16)
+                o_copy(st, i).start()
+
+    def far_wait(st):
+        size = span if st == 0 else 2 * depth
+        start = (1 - side) * span if st == 0 else (door if st == 1 else 3 * side) * size
+        block = far_in.at[:, pl.ds(pl.multiple_of(start, size), size)]
+        remote(block, block, o_send.at[st, 0], o_recv.at[st], {"tp": 1 - p}).wait_recv()
+
+    def ready(t):
+        g_copy(2, t).wait_recv()
 
     for t in near + [(0, 0)]:
-        g_copy(2, t).wait_recv()
-    here, near_first, far_first, drain_first = stage(0, lambda i: None)
-    for t in far:
-        pass_on(2, t)
-    for t in far:
-        g_copy(2, t).wait_recv()
-    there, near_last, far_last, drain_last = stage(1, lambda i: None)
-    near_first()
-    acc = jnp.dot(near_w[...], back[:, here], preferred_element_type=f32)
-    near_last()
-    more = jnp.dot(near_w[...], back[:, there], preferred_element_type=f32)
-    far_first()
-    mixed[:, there] = (more + far_in[:, there].astype(f32)).astype(bf16)
-    far_last()
-    mixed[:, here] = (acc + far_in[:, here].astype(f32)).astype(bf16)
-
-    drain_first()
-    drain_last()
+        ready(t)
+    stage(0)
+    pass_on(2, (2, 0))
+    pass_on(2, (2, 1))
+    ready((2, 0))
+    ready((2, 1))
+    stage(1)
+    pass_on(2, (3, 0))
+    pass_on(2, (3, 1))
+    merge(0)
+    ready((3, 0))
+    ready((3, 1))
+    stage(2)
+    for st in range(3):
+        n_copy(st, (1, 0)).start()
+        n_copy(st, (1, 1)).start()
+    merge(1)
+    merge(2)
+    for t in near:
+        n_copy(0, t).wait_recv()
+    acc = jnp.dot(near_w[...], back[:, here(0)], preferred_element_type=f32)
+    far_wait(0)
+    for st in (1, 2):
+        for t in near:
+            n_copy(st, t).wait_recv()
+        more = jnp.dot(near_w[...], back[:, here(st)], preferred_element_type=f32)
+        mixed[:, here(st)] = (more + far_in[:, here(st)].astype(f32)).astype(bf16)
+    far_wait(1)
+    far_wait(2)
+    mixed[:, here(0)] = (acc + far_in[:, here(0)].astype(f32)).astype(bf16)
+    for st in range(3):
+        for s in order:
+            p_copy(st, s).wait_send()
+        for t in near:
+            n_copy(st, t).wait_send()
+        for t in far:
+            if t[1]:
+                c_copy(st, t).wait_send()
     for t in near + far:
-        key_copy(t).wait_send()
-        tp_copy(peer(t)).wait_send()
+        tp_copy(t).wait_send()
     for w in range(3):
         for t in near + far:
             w_copy(w, t).wait_send()
         for t in near + far + [(0, 0)]:
             g_copy(w, t).wait_send()
-    line_copy(f, 0, level(1) * 2 + y).wait_send()
-    line_copy(f, 1, (2 - side) * 2 + y).wait_send()
-    for t in [(0, 0), (1, 0), (2, 0), (3, 0)]:
-        y_copy(peer(t)).wait_send()
+    for s in range(1, 4):
+        key_copy(s).wait_send()
+    for s in range(4):
+        y_copy(s).wait_send()
+    row_copy(1).wait_send()
+    row_copy(2).wait_send()
 
     @pl.when(is_door)
     def _():
-        for i, t in enumerate([(2, 0), (3, 0)]):
-            line_copy(peer(t), 2 + i, level(1) * 2 + y).wait_send()
+        end_copy(2).wait_send()
+        end_copy(3).wait_send()
+        for st in range(3):
+            for i in range(2):
+                o_copy(st, i).wait_send()
+
+    @pl.when(z != door)
+    def _():
+        for st in range(3):
+            c_copy(st, (2, 0)).wait_send()
+            c_copy(st, (3, 0)).wait_send()
 
 
 def run_handover(sizes, slots, tokens, norm_gain, gate_train, up_train, down_train, expert_ids, route_score):
@@ -575,16 +655,17 @@
         scratch_shapes=[
             pltpu.VMEM((n_fs, depth, hid), f32), pltpu.VMEM((n_fs, depth, hid), f32), pltpu.VMEM((n_fs, hid, depth), f32),
             pltpu.VMEM((n_fs, depth, hid), bf16), pltpu.VMEM((n_fs, depth, hid), bf16), pltpu.VMEM((n_fs, hid, depth), bf16),
-            pltpu.VMEM((n_fs, count, width), bf16), pltpu.VMEM((n_fs, 8, count), f32),
+            pltpu.VMEM((count, width), bf16), pltpu.VMEM((3, count, half), bf16), pltpu.VMEM((n_fs, 8, count), f32),
+            pltpu.VMEM((4, slots, half), bf16),
             pltpu.VMEM((n_fs * slots, width), bf16), pltpu.VMEM((n_fs * slots, hid), bf16),
             pltpu.VMEM((n_fs * slots, width), bf16), pltpu.VMEM((n_fs * slots, half), bf16),
             pltpu.VMEM((n_fs * slots, half), bf16), pltpu.VMEM((quad * slots, half), bf16),
             pltpu.VMEM((2, quad * slots, half), bf16), pltpu.VMEM((2, count, half), bf16), pltpu.VMEM((count, half), bf16),
             pltpu.VMEM((count, quad * slots), bf16), pltpu.VMEM((2, count, quad * slots), bf16),
-            dma((3,)), dma((3, n_fs)), dma((3, n_fs)), dma((3, n_fs)), dma((3, n_fs)), dma((n_fs,)), dma((4,)), dma((n_fs,)),
-            dma((n_fs,)), dma((n_fs,)), dma((n_fs,)), dma((n_fs,)),
-            dma((2, 4)), dma((2, 4)), dma((2, n_fs)), dma((2, n_fs)), dma((2, n_fs)), dma((2, 2, quad)),
-            dma((2, 2)), dma((2,)),
+            dma((3,)), dma((3, n_fs)), dma((3, n_fs)), dma((3, n_fs)), dma((3, n_fs)), dma((4,)), dma((3,)), dma((4,)), dma((4,)),
+            dma((n_fs,)), dma((n_fs,)), dma((4,)), dma((4,)),
+            dma((3, 4)), dma((3, 4)), dma((3, n_fs)), dma((3, n_fs)), dma((3, n_fs)), dma((3, 2, quad)),
+            dma((3, 2)), dma((3,)),
         ],
         compiler_params=pltpu.CompilerParams(collective_id=2, has_side_effects=True, vmem_limit_bytes=54 * 2**20),
         name="handover",

time: 207 us -> 143 us (0.69)
  Pallas kernels: 199 us -> 137 us
    pallas_call x1, Pallas kernels: 199 us -> 137 us  [run_handover(): pl.pallas_call(functools.partial(handover_kernel, sizes), out_shape=(pltp...]
where the time goes in v2:
time: 143 us
  Pallas kernels  137 us (96%)
  local copies, waits for them, and re-layouts  4.75 us (3%)
    pallas_call x1, Pallas kernels, run_handover(): pl.pallas_call(functools.partial(handover_kernel, sizes), out_shape=(pltp...  137 us
    unnamed x4, local copies, waits for them, and re-layouts  4.75 us

profile of v2, /device:TPU:0, one launch (start us, length us, event | category | flops | bytes accessed | tf_op | source)
XLA Modules:
  0.0 142.8 jit_solution(8611810714321250476)
XLA Ops:
  0.6 137.4 %handover.1 = (bf16[1,2048,512]{2,1,0:T(8,128)(2,1)S(1)}, bf16[1,2048,512]{2,1,0:T(8,128)(2,1)S(1)}, bf16[1,512,2048]{2,1,0:T(8,128)(2,1)S(1)}, bf16[256,1024]{1,0:T(8,128)(2,1)S(1)}) custom-call(bf16[256,2048]{1,0:T(8,128)(2,1)} %tokens.1, f32[1,128]{1,0:T(1,128)} %bitcast.5, s32[2,256]{1,0:T(2,128)} %bitcast.3, f32[2,256]{1,0:T(2,128)} %bitcast.4, ...), custom_call_target="tpu_custom_call" | custom-call | tf_op jit(solution)/shard_map/handover/pallas_call | solution.py:645
  138.0 1.3 copy.15
  139.4 0.8 copy.18
  140.2 1.3 copy.16
  141.5 1.3 copy.17

commit v3 on v2

--- a/solution.py
+++ b/solution.py
@@ -224,11 +224,10 @@
             f_copy(k).wait_send()
 
 
-def handover_kernel(sizes, tokens, gain, ids, score, gate_hbm, up_hbm, down_hbm, gate_out, up_out, down_out, mixed,
-                    gate_raw, up_raw, down_raw, gate_cut, up_cut, down_cut, rows_own, line_in, meta, y_pick, picked, hidden,
-                    part, held, total, back, collect, far_out, far_in, near_w, gate_w,
-                    load_sem, w_send, w_recv, g_send, g_recv, x_send, x_recv, y_send, y_recv, t_send, t_recv, k_send, k_recv,
-                    p_send, p_recv, n_send, n_recv, c_send, c_recv, o_send, o_recv):
+def handover_kernel(sizes, tokens_hbm, gain_hbm, ids_hbm, score_hbm, gate_hbm, up_hbm, down_hbm, gate_out, up_out, down_out, mixed,
+                    tokens, gain, ids, score, gate_raw, up_raw, down_raw, gate_cut, up_cut, down_cut, rows_own, line_in, meta, y_pick,
+                    picked, hidden, part, held, total, back, collect, far_out, far_in, near_w, gate_w,
+                    load_sem, w_send, w_recv, g_send, g_recv, d_recv, x_send, x_recv, y_recv, k_recv, p_recv, n_recv, c_recv, o_recv):
     n_fs = sizes["fs"]
     g, f, p = lax.axis_index("gr"), lax.axis_index("fs"), lax.axis_index("tp")
     z, y = f // 2, lax.rem(f, 2)
@@ -241,14 +240,29 @@
     slots = back.shape[0] * 2 // n_fs
     half = width // 2
     span = half // 2
+    strip = 2 * depth
     quad = n_fs // 2
     bf16, f32 = jnp.bfloat16, jnp.float32
     raws, cuts, outs = (gate_raw, up_raw, down_raw), (gate_cut, up_cut, down_cut), (gate_out, up_out, down_out)
     hbms = (gate_hbm, up_hbm, down_hbm)
     near = [(0, 1), (1, 0), (1, 1)]
     far = [(2, 0), (2, 1), (3, 0), (3, 1)]
-    index = {t: i for i, t in enumerate(near + far + [(0, 0)])}
+    index = {t: i for i, t in enumerate(near + far)}
     mine = lax.rem(f, quad)
+    rows_send, relay_send, y_send, t_send, k_send, p_send, n_send, c_send, e_send, o_send, t_recv = [x_send.at[i] for i in range(11)]
+
+    def at_door(act, otherwise=None):
+        @pl.when(is_door)
+        def _():
+            act()
+
+        if otherwise is not None:
+            at_end(otherwise)
+
+    def at_end(act):
+        @pl.when(z != door)
+        def _():
+            act()
 
     def level(s):
         return (z, z + 1 - 2 * low, 2 - side, 3 - 3 * side)[s]
@@ -272,49 +286,47 @@
         at = pl.ds(pl.multiple_of(block * depth, depth), depth)
         return outs[w].at[0, at, :] if w < 2 else outs[w].at[0, :, at]
 
+    def local(block, send, recv):
+        return remote(block, block, send, recv, {"tp": 1 - p})
+
     def w_copy(w, t):
         to = peer(t)
-        return remote(cuts[w].at[to], place(w, g * n_fs + f), w_send.at[w, index[t]], w_recv.at[w, there(t)], {"fs": to})
-
-    def w_wait(w, t):
-        block = place(w, g * n_fs + peer(t))
-        remote(block, block, w_send.at[w, index[t]], w_recv.at[w, index[t]], {"fs": peer(t)}).wait_recv()
+        return remote(cuts[w].at[to], place(w, g * n_fs + f), w_send.at[w], w_recv.at[w, there(t)], {"fs": to})
 
     def g_copy(w, t):
         b = g * n_fs + peer(t)
         src = cuts[w].at[f] if t == (0, 0) else place(w, b)
-        return remote(src, place(w, b), g_send.at[w, index[t]], g_recv.at[w, index[t]], {"gr": 1 - g})
-
-    def pass_on(w, t):
-        w_wait(w, t)
-        g_copy(w, t).start()
+        return remote(src, place(w, b), g_send.at[w], g_recv.at[w] if w < 2 else d_recv.at[t[0]], {"gr": 1 - g})
+
+    def pass_on(w, *ts):
+        for t in ts:
+            local(place(w, g * n_fs + peer(t)), w_send.at[w], w_recv.at[w, index[t]]).wait_recv()
+            g_copy(w, t).start()
+
+    def ready(s):
+        local(down_out.at[0, :, pl.ds(0, strip)], g_send.at[2], d_recv.at[s]).wait_recv()
 
     def row_copy(s):
         if s == 1:
-            return remote(rows_own.at[:, cols(p)], line_in.at[0], x_send.at[0], x_recv.at[0], {"fs": peer((1, 0))})
-        return remote(rows_own.at[:, cols(p)], line_in.at[1 + role], x_send.at[1], x_recv.at[1 + role], {"fs": peer((2, 0))})
-
-    def end_copy(s):
-        return remote(line_in.at[s - 1], line_in.at[s - 1], x_send.at[s], x_recv.at[s - 1], {"fs": peer((1, 0))})
+            return remote(rows_own.at[:, cols(p)], line_in.at[0], rows_send, x_recv.at[0], {"fs": peer((1, 0))})
+        return remote(rows_own.at[:, cols(p)], line_in.at[1 + role], rows_send, x_recv.at[1 + role], {"fs": peer((2, 0))})
+
+    def relay_copy(s):
+        return remote(line_in.at[s - 1], line_in.at[s - 1], relay_send, x_recv.at[s - 1], {"fs": peer((1, 0))})
 
     def y_copy(s):
-        return remote(y_pick.at[s], picked.at[seat(peer((s, 0))), cols(p)], y_send.at[s], y_recv.at[s], {"fs": peer((0, 1))})
-
-    def y_wait(s):
-        block = picked.at[seat(peer((s, 1))), cols(p)]
-        remote(block, block, y_send.at[s], y_recv.at[s], {"fs": peer((0, 1))}).wait_recv()
+        return remote(y_pick.at[s], picked.at[seat(peer((s, 0))), cols(p)], y_send, y_recv.at[s], {"fs": peer((0, 1))})
 
     def tp_copy(t):
         block = picked.at[seat(peer(t)), cols(p)]
-        return remote(block, block, t_send.at[index[t]], t_recv.at[index[t]], {"tp": 1 - p})
+        return remote(block, block, t_send, t_recv, {"tp": 1 - p})
+
+    def take_y(s):
+        local(picked.at[seat(peer((s, 1))), cols(p)], y_send, y_recv.at[s]).wait_recv()
+        tp_copy((s, 1)).start()
 
     def key_copy(s):
-        to = s if s < 2 else 2 + role
-        return remote(meta.at[f], meta.at[f], k_send.at[s], k_recv.at[to], {"fs": peer((s, 0))})
-
-    def key_wait(s):
-        block = meta.at[peer((s, 0))]
-        remote(block, block, k_send.at[s], k_recv.at[s], {"fs": peer((s, 0))}).wait_recv()
+        return remote(meta.at[f], meta.at[f], k_send, k_recv.at[s if s < 2 else 2 + role], {"fs": peer((s, 0))})
 
     def cut(w):
         pltpu.make_async_copy(hbms[w], raws[w], load_sem.at[w]).wait()
@@ -341,19 +353,16 @@
         return table.T.astype(bf16)
 
     def take_line(s, relay):
-        arriving = remote(line_in.at[s - 1], line_in.at[s - 1], x_send.at[0], x_recv.at[s - 1], {"fs": peer((1, 0))})
-        arriving.wait_recv()
+        local(line_in.at[s - 1], rows_send, x_recv.at[s - 1]).wait_recv()
         if relay:
-            end_copy(s).start()
+            relay_copy(s).start()
         b = peer((s, 0))
-        key_wait(s)
+        local(meta.at[b], k_send, k_recv.at[s]).wait_recv()
         y_pick[s] = pick(b, peer((0, 1)), line_in[s - 1])
         picked[seat(b), cols(p)] = pick(b, f, line_in[s - 1])
         y_copy(s).start()
         tp_copy((s, 0)).start()
 
-    for w in range(3):
-        pltpu.make_async_copy(hbms[w], raws[w], load_sem.at[w]).start()
     barrier = pltpu.get_barrier_semaphore()
     heard = 0
     for name, size in sizes.items():
@@ -361,7 +370,14 @@
         for k in range(1, size):
             pl.semaphore_signal(barrier, inc=1, device_id={name: lax.rem(me + k, size)}, device_id_type=MESH)
             heard += 1
-
+    loads = [pltpu.make_async_copy(src, dst, load_sem.at[3 + i]) for i, (src, dst) in enumerate(
+        [(ids_hbm, ids), (score_hbm, score), (tokens_hbm, tokens), (gain_hbm, gain)])]
+    for c in loads:
+        c.start()
+    for w in range(3):
+        pltpu.make_async_copy(hbms[w], raws[w], load_sem.at[w]).start()
+    loads[0].wait()
+    loads[1].wait()
     expert = lax.broadcasted_iota(jnp.int32, (16, count), 0)
     names = ((ids[0:1, :] == expert) | (ids[1:2, :] == expert)).astype(f32).astype(bf16)
     earlier = lax.broadcasted_iota(jnp.int32, (count, count), 0) < lax.broadcasted_iota(jnp.int32, (count, count), 1)
@@ -372,6 +388,8 @@
     for i in range(4):
         meta[f, i:i + 1, :] = table[i]
     meta[f, 4:8, :] = jnp.zeros((4, count), f32)
+    loads[2].wait()
+    loads[3].wait()
     for r in range(0, count, 32):
         x = tokens[r:r + 32, :].astype(f32)
         rows_own[r:r + 32, :] = (x * lax.rsqrt(jnp.mean(x * x, axis=-1, keepdims=True) + epsilon)).astype(bf16)
@@ -395,90 +413,53 @@
     w_copy(2, (0, 1)).start()
     g_copy(2, (0, 0)).start()
 
-    @pl.when(z != door)
-    def _():
+    def early_down():
         w_copy(2, (1, 0)).start()
         w_copy(2, (1, 1)).start()
 
+    at_end(early_down)
     for c in range(0, width, 512):
         picked[seat(f), c:c + 512] = pick(f, f, rows_own[:, c:c + 512])
     near_w[...] = shares(f)
-    y_wait(0)
-    tp_copy((0, 1)).start()
+    take_y(0)
     pass_on(0, (0, 1))
     pass_on(1, (0, 1))
     take_line(1, False)
-
-    @pl.when(is_door)
-    def _():
-        take_line(2, True)
-
-    pass_on(0, (1, 0))
-    pass_on(0, (1, 1))
-
-    @pl.when(is_door)
-    def _():
-        take_line(3, True)
-
-    pass_on(1, (1, 0))
-    pass_on(1, (1, 1))
-
-    @pl.when(is_door)
-    def _():
+    at_door(lambda: take_line(2, True))
+    pass_on(0, (1, 0), (1, 1))
+    at_door(lambda: take_line(3, True))
+    pass_on(1, (1, 0), (1, 1))
+
+    def gate_shares():
         for i in range(2):
             gate_w[i] = shares(peer((2 + i, 0)))
 
-    pass_on(0, (3, 0))
-    pass_on(0, (3, 1))
+    at_door(gate_shares)
+    pass_on(0, (3, 0), (3, 1))
     pass_on(0, (2, 0))
-    pass_on(0, (2, 1))
-    y_wait(1)
-    tp_copy((1, 1)).start()
-
-    @pl.when(z != door)
-    def _():
-        take_line(2, False)
-
-
-    @pl.when(is_door)
-    def _():
-        for s in (2, 3):
-            y_wait(s)
-            tp_copy((s, 1)).start()
-
+    at_end(lambda: take_line(2, False))
+    at_door(lambda: pass_on(0, (2, 1)))
+    take_y(1)
+
+    def take_both():
+        take_y(2)
+        take_y(3)
+
+    at_door(take_both)
     pass_on(2, (0, 1))
-    pass_on(1, (3, 0))
-    pass_on(1, (3, 1))
-
-    @pl.when(z != door)
-    def _():
-        take_line(3, False)
-        y_wait(2)
-        tp_copy((2, 1)).start()
-
-    pass_on(1, (2, 0))
-    pass_on(1, (2, 1))
-
-    @pl.when(is_door)
-    def _():
-        w_copy(2, (1, 0)).start()
-        w_copy(2, (1, 1)).start()
-
+    pass_on(1, (3, 0), (3, 1))
+    at_end(lambda: pass_on(0, (2, 1)))
+    at_end(lambda: take_line(3, False))
+    at_end(lambda: take_y(2))
+    pass_on(1, (2, 0), (2, 1))
+    at_door(early_down)
     for t in far:
         w_copy(2, t).start()
-
-    @pl.when(z != door)
-    def _():
-        y_wait(3)
-        tp_copy((3, 1)).start()
-
-    for t in near[1:]:
-        pass_on(2, t)
-    for t in near + far:
-        tp_copy(t).wait_recv()
+    at_end(lambda: take_y(3))
+    at_door(lambda: pass_on(2, (1, 0), (1, 1)))
+    local(picked.at[pl.ds(0, (n_fs - 1) * slots), pl.ds(0, half)], t_send, t_recv).wait_recv()
     for w in range(2):
-        for t in near + far + [(0, 0)]:
-            g_copy(w, t).wait_recv()
+        local(outs[w].at[0, pl.ds(0, n_fs * depth), :], g_send.at[w], g_recv.at[w]).wait_recv()
     order = [2, 3, 1, 0]
 
     def act(s):
@@ -487,152 +468,139 @@
         hidden[pair(s), :] = (gate_act / (1.0 + jnp.exp(-gate_act)) * up_act).astype(bf16)
 
     def here(st, base=0):
-        size = span if st == 0 else 2 * depth
-        return pl.ds(pl.multiple_of(base + (side * span if st == 0 else level(1 + st) * (2 * depth)), size), size)
+        layer = (3 * side, door, 2 - side, 3 - 3 * side)[st]
+        return pl.ds(pl.multiple_of(base + layer * strip, strip), strip)
 
     def p_copy(st, s):
-        return remote(part.at[pair(s), here(st, (1 - p) * half)], held.at[pair(s), here(st)], p_send.at[st, s], p_recv.at[st, s],
-                      {"tp": 1 - p})
+        return remote(part.at[pair(s), here(st, (1 - p) * half)], held.at[pair(s), here(st)], p_send, p_recv.at[st, s], {"tp": 1 - p})
 
     def n_copy(st, t):
-        return remote(total.at[seat(peer(t)), here(st)], back.at[seat(mine), here(st)], n_send.at[st, index[t]],
-                      n_recv.at[st, index[t]], {"fs": peer(t)})
+        return remote(total.at[seat(peer(t)), here(st)], back.at[seat(mine), here(st)], n_send, n_recv.at[max(st - 1, 0)],
+                      {"fs": peer(t)})
 
     def c_copy(st, t):
-        return remote(total.at[seat(peer(t)), here(st)], collect.at[t[0] - 2, seat(mine), here(st)], c_send.at[st, index[t]],
-                      c_recv.at[st, t[0] - 2, mine], {"fs": door * 2 + (1 - y if t[1] else y)})
+        return remote(total.at[seat(peer(t)), here(st)], collect.at[t[0] - 2, seat(mine), here(st)], c_send if t[1] else e_send,
+                      c_recv.at[st, t[0] - 2], {"fs": door * 2 + (1 - y if t[1] else y)})
 
     def o_copy(st, i):
-        return remote(far_out.at[i, :, here(st)], far_in.at[:, here(st)], o_send.at[st, i], o_recv.at[st], {"fs": peer((2 + i, 0))})
-
-    def stage(st):
-        def compute(s):
+        return remote(far_out.at[i, :, here(st)], far_in.at[:, here(st)], o_send, o_recv.at[st], {"fs": peer((2 + i, 0))})
+
+    def compute(st):
+        for i, s in enumerate(order):
+            if st == 0:
+                act(s)
             for q in range(2):
                 part[pair(s), here(st, q * half)] = jnp.dot(
                     hidden[pair(s), :], down_out[0, :, here(st, q * half)], preferred_element_type=f32).astype(bf16)
-
-        def add(s):
-            p_copy(st, s).wait_recv()
-            total[pair(s), here(st)] = (part[pair(s), here(st, p * half)].astype(f32) + held[pair(s), here(st)].astype(f32)).astype(bf16)
-
-        def give(s):
+            if i:
+                p_copy(st, order[i - 1]).start()
+        p_copy(st, order[-1]).start()
+
+    def give(st):
+        def send(s):
             for dy in range(2):
                 t = (s, dy)
                 if t == (0, 0):
                     back[seat(mine), here(st)] = total[seat(f), here(st)]
                 elif s == 0:
                     n_copy(st, t).start()
-                elif s == 1:
-                    pass
-                elif dy:
+                elif dy and s > 1:
                     c_copy(st, t).start()
-                else:
-                    @pl.when(is_door)
-                    def _():
+                elif s > 1:
+                    def keep():
                         collect[s - 2, seat(mine), here(st)] = total[seat(peer(t)), here(st)]
 
-                    @pl.when(z != door)
-                    def _():
-                        c_copy(st, t).start()
-
-        for i in range(len(order) + 3):
-            if i < len(order):
-                if st == 0:
-                    act(order[i])
-                compute(order[i])
-            if 0 <= i - 1 < len(order):
-                p_copy(st, order[i - 1]).start()
-            if 0 <= i - 2 < len(order):
-                add(order[i - 2])
-            if 0 <= i - 3 < len(order):
-                give(order[i - 3])
+                    at_door(keep, lambda: c_copy(st, t).start())
+
+        for i, s in enumerate(order):
+            p_copy(st, s).wait_recv()
+            total[pair(s), here(st)] = (part[pair(s), here(st, p * half)].astype(f32) + held[pair(s), here(st)].astype(f32)).astype(bf16)
+            if i:
+                send(order[i - 1])
+        send(order[-1])
+
+    def give_near(st):
+        n_copy(st, (1, 0)).start()
+        n_copy(st, (1, 1)).start()
 
     def merge(st):
-        @pl.when(is_door)
-        def _():
+        def act():
             for i in range(2):
-                for k in range(1, quad):
-                    j = lax.rem(mine + k, quad)
-                    block = collect.at[i, seat(j), here(st)]
-                    remote(block, block, c_send.at[st, 0], c_recv.at[st, i, j], {"tp": 1 - p}).wait_recv()
+                local(collect.at[i, pl.ds(0, (quad - 1) * slots), here(st)], c_send, c_recv.at[st, i]).wait_recv()
                 far_out[i, :, here(st)] = jnp.dot(gate_w[i], collect[i, :, here(st)], preferred_element_type=f32).astype(bf16)
                 o_copy(st, i).start()
 
+        at_door(act)
+
     def far_wait(st):
-        size = span if st == 0 else 2 * depth
-        start = (1 - side) * span if st == 0 else (door if st == 1 else 3 * side) * size
-        block = far_in.at[:, pl.ds(pl.multiple_of(start, size), size)]
-        remote(block, block, o_send.at[st, 0], o_recv.at[st], {"tp": 1 - p}).wait_recv()
-
-    def ready(t):
-        g_copy(2, t).wait_recv()
-
-    for t in near + [(0, 0)]:
-        ready(t)
-    stage(0)
-    pass_on(2, (2, 0))
-    pass_on(2, (2, 1))
-    ready((2, 0))
-    ready((2, 1))
-    stage(1)
-    pass_on(2, (3, 0))
-    pass_on(2, (3, 1))
+        layer = (3 - 3 * side, 2 - side, door, 3 * side)[st]
+        local(far_in.at[:, pl.ds(pl.multiple_of(layer * strip, strip), strip)], o_send, o_recv.at[st]).wait_recv()
+
+    at_door(lambda: ready(1), lambda: ready(0))
+    compute(0)
+    give(0)
+
+    def late_down():
+        pass_on(2, (1, 0), (1, 1))
+        ready(1)
+
+    at_door(lambda: ready(0), late_down)
+    compute(1)
+    pass_on(2, (2, 0), (2, 1))
+    give(1)
+    give_near(0)
+    give_near(1)
     merge(0)
-    ready((3, 0))
-    ready((3, 1))
-    stage(2)
-    for st in range(3):
-        n_copy(st, (1, 0)).start()
-        n_copy(st, (1, 1)).start()
+    pass_on(2, (3, 0), (3, 1))
+    ready(2)
+    compute(2)
     merge(1)
+    give(2)
+    ready(3)
+    compute(3)
+    give(3)
+    give_near(2)
+    give_near(3)
     merge(2)
-    for t in near:
-        n_copy(0, t).wait_recv()
-    acc = jnp.dot(near_w[...], back[:, here(0)], preferred_element_type=f32)
+    merge(3)
+    local(back.at[pl.ds(0, 3 * slots // 2), :], n_send, n_recv.at[0]).wait_recv()
+    sided = pl.ds(pl.multiple_of(side * span, span), span)
+    acc = jnp.dot(near_w[...], back[:, sided], preferred_element_type=f32)
     far_wait(0)
-    for st in (1, 2):
-        for t in near:
-            n_copy(st, t).wait_recv()
+    far_wait(1)
+    for st in (2, 3):
+        local(back.at[pl.ds(0, 3 * slots // 4), :], n_send, n_recv.at[st - 1]).wait_recv()
         more = jnp.dot(near_w[...], back[:, here(st)], preferred_element_type=f32)
         mixed[:, here(st)] = (more + far_in[:, here(st)].astype(f32)).astype(bf16)
-    far_wait(1)
     far_wait(2)
-    mixed[:, here(0)] = (acc + far_in[:, here(0)].astype(f32)).astype(bf16)
-    for st in range(3):
-        for s in order:
-            p_copy(st, s).wait_send()
-        for t in near:
-            n_copy(st, t).wait_send()
-        for t in far:
-            if t[1]:
-                c_copy(st, t).wait_send()
-    for t in near + far:
-        tp_copy(t).wait_send()
+    far_wait(3)
+    mixed[:, sided] = (acc + far_in[:, sided].astype(f32)).astype(bf16)
+
+    def sent(block, send):
+        local(block, send, o_recv.at[0]).wait_send()
+
     for w in range(3):
-        for t in near + far:
-            w_copy(w, t).wait_send()
-        for t in near + far + [(0, 0)]:
-            g_copy(w, t).wait_send()
-    for s in range(1, 4):
-        key_copy(s).wait_send()
-    for s in range(4):
-        y_copy(s).wait_send()
-    row_copy(1).wait_send()
-    row_copy(2).wait_send()
-
-    @pl.when(is_door)
-    def _():
-        end_copy(2).wait_send()
-        end_copy(3).wait_send()
-        for st in range(3):
-            for i in range(2):
-                o_copy(st, i).wait_send()
-
-    @pl.when(z != door)
-    def _():
-        for st in range(3):
-            c_copy(st, (2, 0)).wait_send()
-            c_copy(st, (3, 0)).wait_send()
+        sent(cuts[w].at[pl.ds(0, n_fs - 1)], w_send.at[w])
+        sent(cuts[w], g_send.at[w])
+    sent(rows_own, rows_send)
+    sent(y_pick, y_send)
+    sent(picked.at[pl.ds(0, (n_fs - 1) * slots), pl.ds(0, half)], t_send)
+    sent(meta.at[pl.ds(0, 3)], k_send)
+    sent(held, p_send)
+    sent(held.at[pl.ds(0, 3 * slots), :], n_send)
+    sent(held.at[pl.ds(0, 2 * slots), :], c_send)
+    at_door(lambda: sent(line_in.at[pl.ds(0, 2)], relay_send), lambda: sent(held.at[pl.ds(0, 2 * slots), :], e_send))
+    at_door(lambda: sent(far_out, o_send))
+
+
+def store_kernel(*refs):
+    sems = refs[-1]
+    pairs = list(zip(refs[:4], refs[4:8]))
+    copies = [pltpu.make_async_copy(src, dst, sems.at[i]) for i, (src, dst) in enumerate(pairs)]
+    for c in copies:
+        c.start()
+    for c in copies:
+        c.wait()
 
 
 def run_handover(sizes, slots, tokens, norm_gain, gate_train, up_train, down_train, expert_ids, route_score):
@@ -641,18 +609,15 @@
     count, width = tokens.shape
     half, quad = width // n_tp, n_fs // 2
     bf16, f32, dma = jnp.bfloat16, jnp.float32, pltpu.SemaphoreType.DMA
-    vmem, hbm = pl.BlockSpec(memory_space=pltpu.VMEM), pl.BlockSpec(memory_space=pl.ANY)
-    return pl.pallas_call(
+    vmem, hbm = pl.BlockSpec(memory_space=pltpu.VMEM), pl.BlockSpec(memory_space=pltpu.HBM)
+    shapes = [(1, width, hid), (1, width, hid), (1, hid, width), (count, half)]
+    made = pl.pallas_call(
         functools.partial(handover_kernel, sizes),
-        out_shape=(
-            pltpu.VMEM((1, width, hid), bf16),
-            pltpu.VMEM((1, width, hid), bf16),
-            pltpu.VMEM((1, hid, width), bf16),
-            pltpu.VMEM((count, half), bf16),
-        ),
-        in_specs=[vmem] * 4 + [hbm] * 3,
+        out_shape=[pltpu.VMEM(shape, bf16) for shape in shapes],
+        in_specs=[hbm] * 7,
         out_specs=[vmem] * 4,
         scratch_shapes=[
+            pltpu.VMEM((count, width), bf16), pltpu.VMEM((1, depth), f32), pltpu.VMEM((2, count), jnp.int32), pltpu.VMEM((2, count), f32),
             pltpu.VMEM((n_fs, depth, hid), f32), pltpu.VMEM((n_fs, depth, hid), f32), pltpu.VMEM((n_fs, hid, depth), f32),
             pltpu.VMEM((n_fs, depth, hid), bf16), pltpu.VMEM((n_fs, depth, hid), bf16), pltpu.VMEM((n_fs, hid, depth), bf16),
             pltpu.VMEM((count, width), bf16), pltpu.VMEM((3, count, half), bf16), pltpu.VMEM((n_fs, 8, count), f32),
@@ -662,14 +627,21 @@
             pltpu.VMEM((n_fs * slots, half), bf16), pltpu.VMEM((quad * slots, half), bf16),
             pltpu.VMEM((2, quad * slots, half), bf16), pltpu.VMEM((2, count, half), bf16), pltpu.VMEM((count, half), bf16),
             pltpu.VMEM((count, quad * slots), bf16), pltpu.VMEM((2, count, quad * slots), bf16),
-            dma((3,)), dma((3, n_fs)), dma((3, n_fs)), dma((3, n_fs)), dma((3, n_fs)), dma((4,)), dma((3,)), dma((4,)), dma((4,)),
-            dma((n_fs,)), dma((n_fs,)), dma((4,)), dma((4,)),
-            dma((3, 4)), dma((3, 4)), dma((3, n_fs)), dma((3, n_fs)), dma((3, n_fs)), dma((3, 2, quad)),
-            dma((3, 2)), dma((3,)),
+            dma((7,)), dma((3,)), dma((3, n_fs - 1)), dma((3,)), dma((2,)), dma((4,)), dma((11,)), dma((3,)), dma((4,)), dma((4,)),
+            dma((4, 4)), dma((3,)), dma((4, 2)), dma((4,)),
         ],
-        compiler_params=pltpu.CompilerParams(collective_id=2, has_side_effects=True, vmem_limit_bytes=54 * 2**20),
+        compiler_params=pltpu.CompilerParams(collective_id=2, has_side_effects=True, vmem_limit_bytes=56 * 2**20),
         name="handover",
     )(tokens, norm_gain.reshape(1, depth), expert_ids.T, route_score.T, gate_train, up_train, down_train)
+    return pl.pallas_call(
+        store_kernel,
+        out_shape=[jax.ShapeDtypeStruct(shape, bf16) for shape in shapes],
+        in_specs=[vmem] * 4,
+        out_specs=[pl.BlockSpec(memory_space=pl.ANY)] * 4,
+        scratch_shapes=[dma((4,))],
+        compiler_params=pltpu.CompilerParams(vmem_limit_bytes=16 * 2**20),
+        name="store",
+    )(*made)
 
 
 def on_device(sizes, tokens, norm_gain, gate_train, up_train, down_train, expert_ids, route_score):

time: 143 us -> 134 us (0.937)
  local copies, waits for them, and re-layouts: 4.75 us -> 0 us
  Pallas kernels: 137 us -> 133 us
    unnamed x4 -> x0, local copies, waits for them, and re-layouts: 4.75 us -> none
    pallas_call x1 -> x2, Pallas kernels: 137 us -> 133 us  [the longest x1 130 us: run_handover(): pl.pallas_call(functools.partial(handover_kernel, sizes), out_shape=[pltp...]
where the time goes in v3:
time: 134 us
  Pallas kernels  133 us (99%)
    pallas_call x1, Pallas kernels, run_handover(): pl.pallas_call(functools.partial(handover_kernel, sizes), out_shape=[pltp...  130 us
    pallas_call x1, Pallas kernels, run_handover(): pl.pallas_call(store_kernel, out_shape=[jax.ShapeDtypeStruct(shape, bf16)...  2.84 us

profile of v3, /device:TPU:0, one launch (start us, length us, event | category | flops | bytes accessed | tf_op | source)
XLA Modules:
  0.0 133.6 jit_solution(13377125384074898961)
XLA Ops:
  0.6 130.1 %handover.1 = (bf16[1,2048,512]{2,1,0:T(8,128)(2,1)S(1)}, bf16[1,2048,512]{2,1,0:T(8,128)(2,1)S(1)}, bf16[1,512,2048]{2,1,0:T(8,128)(2,1)S(1)}, bf16[256,1024]{1,0:T(8,128)(2,1)S(1)}) custom-call(bf16[256,2048]{1,0:T(8,128)(2,1)} %tokens_hbm.1, f32[1,128]{1,0:T(1,128)} %bitcast.5, s32[2,256]{1,0:T(2,128)} %bitcast.3, f32[2,256]{1,0:T(2,128)} %bitcast.4, ...), custom_call_target="tpu_custom_call" | custom-call | tf_op jit(solution)/shard_map/handover/pallas_call | solution.py:614
  130.8 2.8 %store.1 = (bf16[1,2048,512]{2,1,0:T(8,128)(2,1)}, bf16[1,2048,512]{2,1,0:T(8,128)(2,1)}, bf16[1,512,2048]{2,1,0:T(8,128)(2,1)}, bf16[256,1024]{1,0:T(8,128)(2,1)}) custom-call(bf16[1,2048,512]{2,1,0:T(8,128)(2,1)S(1)} %get-tuple-element.8.refs_0_, bf16[1,2048,512]{2,1,0:T(8,128)(2,1)S(1)} %get-tuple-element.9.refs_1_, ...), custom_call_target="tpu_custom_call" | custom-call | tf_op jit(solution)/shard_map/store/pallas_call | solution.py:636

commit v4 on v3

--- a/solution.py
+++ b/solution.py
@@ -226,8 +226,8 @@
 
 def handover_kernel(sizes, tokens_hbm, gain_hbm, ids_hbm, score_hbm, gate_hbm, up_hbm, down_hbm, gate_out, up_out, down_out, mixed,
                     tokens, gain, ids, score, gate_raw, up_raw, down_raw, gate_cut, up_cut, down_cut, rows_own, line_in, meta, y_pick,
-                    picked, hidden, part, held, total, back, collect, far_out, far_in, near_w, gate_w,
-                    load_sem, w_send, w_recv, g_send, g_recv, d_recv, x_send, x_recv, y_recv, k_recv, p_recv, n_recv, c_recv, o_recv):
+                    picked, gate_act, hidden, part, held, total, back, collect, far_out, far_in, near_w, gate_w,
+                    load_sem, w_send, w_recv, g_send, g_recv, d_recv, x_send, x_recv, y_recv, k_recv, t_recv, p_recv, n_recv, c_recv, o_recv):
     n_fs = sizes["fs"]
     g, f, p = lax.axis_index("gr"), lax.axis_index("fs"), lax.axis_index("tp")
     z, y = f // 2, lax.rem(f, 2)
@@ -249,7 +249,7 @@
     far = [(2, 0), (2, 1), (3, 0), (3, 1)]
     index = {t: i for i, t in enumerate(near + far)}
     mine = lax.rem(f, quad)
-    rows_send, relay_send, y_send, t_send, k_send, p_send, n_send, c_send, e_send, o_send, t_recv = [x_send.at[i] for i in range(11)]
+    rows_send, relay_send, y_send, t_send, k_send, p_send, n_send, c_send, e_send, o_send = [x_send.at[i] for i in range(10)]
 
     def at_door(act, otherwise=None):
         @pl.when(is_door)
@@ -319,7 +319,7 @@
 
     def tp_copy(t):
         block = picked.at[seat(peer(t)), cols(p)]
-        return remote(block, block, t_send, t_recv, {"tp": 1 - p})
+        return remote(block, block, t_send, t_recv.at[t[0]], {"tp": 1 - p})
 
     def take_y(s):
         local(picked.at[seat(peer((s, 1))), cols(p)], y_send, y_recv.at[s]).wait_recv()
@@ -362,6 +362,14 @@
         picked[seat(b), cols(p)] = pick(b, f, line_in[s - 1])
         y_copy(s).start()
         tp_copy((s, 0)).start()
+
+    def whole(w):
+        local(outs[w].at[0, pl.ds(0, n_fs * depth), :], g_send.at[w], g_recv.at[w]).wait_recv()
+
+    def gate_of(s):
+        blocks = 1 if s == 0 else 2
+        local(picked.at[pl.ds(0, blocks * slots), pl.ds(0, half)], t_send, t_recv.at[s]).wait_recv()
+        gate_act[pair(s), :] = jnp.dot(picked[pair(s), :], gate_out[0], preferred_element_type=f32)
 
     barrier = pltpu.get_barrier_semaphore()
     heard = 0
@@ -389,16 +397,16 @@
         meta[f, i:i + 1, :] = table[i]
     meta[f, 4:8, :] = jnp.zeros((4, count), f32)
     loads[2].wait()
-    loads[3].wait()
     for r in range(0, count, 32):
         x = tokens[r:r + 32, :].astype(f32)
         rows_own[r:r + 32, :] = (x * lax.rsqrt(jnp.mean(x * x, axis=-1, keepdims=True) + epsilon)).astype(bf16)
-    y_pick[0] = pick(f, peer((0, 1)), rows_own[:, cols(p)])
     pl.semaphore_wait(barrier, heard)
     for s in range(1, 4):
         key_copy(s).start()
     row_copy(1).start()
     row_copy(2).start()
+    y_pick[0] = pick(f, peer((0, 1)), rows_own[:, cols(p)])
+    loads[3].wait()
     y_copy(0).start()
     cut(0)
     for t in near:
@@ -451,24 +459,30 @@
     at_end(lambda: pass_on(0, (2, 1)))
     at_end(lambda: take_line(3, False))
     at_end(lambda: take_y(2))
+
+    def far_down():
+        for t in far:
+            w_copy(2, t).start()
+
+    whole(0)
+    for s in (1, 0, 2):
+        gate_of(s)
+    at_door(lambda: gate_of(3))
     pass_on(1, (2, 0), (2, 1))
     at_door(early_down)
-    for t in far:
-        w_copy(2, t).start()
+    far_down()
     at_end(lambda: take_y(3))
     at_door(lambda: pass_on(2, (1, 0), (1, 1)))
-    local(picked.at[pl.ds(0, (n_fs - 1) * slots), pl.ds(0, half)], t_send, t_recv).wait_recv()
-    for w in range(2):
-        local(outs[w].at[0, pl.ds(0, n_fs * depth), :], g_send.at[w], g_recv.at[w]).wait_recv()
+    whole(1)
     order = [2, 3, 1, 0]
 
     def act(s):
-        gate_act = jnp.dot(picked[pair(s), :], gate_out[0], preferred_element_type=f32)
+        gated = gate_act[pair(s), :]
         up_act = jnp.dot(picked[pair(s), :], up_out[0], preferred_element_type=f32)
-        hidden[pair(s), :] = (gate_act / (1.0 + jnp.exp(-gate_act)) * up_act).astype(bf16)
+        hidden[pair(s), :] = (gated / (1.0 + jnp.exp(-gated)) * up_act).astype(bf16)
 
     def here(st, base=0):
-        layer = (3 * side, door, 2 - side, 3 - 3 * side)[st]
+        layer = (3 * side, door, 3 - 3 * side, 2 - side)[st]
         return pl.ds(pl.multiple_of(base + layer * strip, strip), strip)
 
     def p_copy(st, s):
@@ -485,39 +499,61 @@
     def o_copy(st, i):
         return remote(far_out.at[i, :, here(st)], far_in.at[:, here(st)], o_send, o_recv.at[st], {"fs": peer((2 + i, 0))})
 
+    def spread(st, s):
+        for q in range(2):
+            part[pair(s), here(st, q * half)] = jnp.dot(
+                hidden[pair(s), :], down_out[0, :, here(st, q * half)], preferred_element_type=f32).astype(bf16)
+
+    def add(st, s):
+        p_copy(st, s).wait_recv()
+        total[pair(s), here(st)] = (part[pair(s), here(st, p * half)].astype(f32) + held[pair(s), here(st)].astype(f32)).astype(bf16)
+
+    def send(st, s):
+        for dy in range(2):
+            t = (s, dy)
+            if t == (0, 0):
+                back[seat(mine), here(st)] = total[seat(f), here(st)]
+            elif s == 0:
+                n_copy(st, t).start()
+            elif dy and s > 1:
+                c_copy(st, t).start()
+            elif s > 1:
+                def keep():
+                    collect[s - 2, seat(mine), here(st)] = total[seat(peer(t)), here(st)]
+
+                at_door(keep, lambda: c_copy(st, t).start())
+
+    def first():
+        for i in range(len(order) + 1):
+            if i < len(order):
+                if order[i] == 3:
+                    at_end(lambda: gate_of(3))
+                act(order[i])
+            if i:
+                add(0, order[i - 1])
+            if i < len(order):
+                spread(0, order[i])
+            if i:
+                send(0, order[i - 1])
+            if i < len(order):
+                p_copy(0, order[i]).start()
+            if i == 0:
+                at_end(lambda: pass_on(2, (1, 0), (1, 1)))
+        give_near(0)
+
     def compute(st):
         for i, s in enumerate(order):
-            if st == 0:
-                act(s)
-            for q in range(2):
-                part[pair(s), here(st, q * half)] = jnp.dot(
-                    hidden[pair(s), :], down_out[0, :, here(st, q * half)], preferred_element_type=f32).astype(bf16)
+            spread(st, s)
             if i:
                 p_copy(st, order[i - 1]).start()
         p_copy(st, order[-1]).start()
 
     def give(st):
-        def send(s):
-            for dy in range(2):
-                t = (s, dy)
-                if t == (0, 0):
-                    back[seat(mine), here(st)] = total[seat(f), here(st)]
-                elif s == 0:
-                    n_copy(st, t).start()
-                elif dy and s > 1:
-                    c_copy(st, t).start()
-                elif s > 1:
-                    def keep():
-                        collect[s - 2, seat(mine), here(st)] = total[seat(peer(t)), here(st)]
-
-                    at_door(keep, lambda: c_copy(st, t).start())
-
         for i, s in enumerate(order):
-            p_copy(st, s).wait_recv()
-            total[pair(s), here(st)] = (part[pair(s), here(st, p * half)].astype(f32) + held[pair(s), here(st)].astype(f32)).astype(bf16)
+            add(st, s)
             if i:
-                send(order[i - 1])
-        send(order[-1])
+                send(st, order[i - 1])
+        send(st, order[-1])
 
     def give_near(st):
         n_copy(st, (1, 0)).start()
@@ -533,34 +569,27 @@
         at_door(act)
 
     def far_wait(st):
-        layer = (3 - 3 * side, 2 - side, door, 3 * side)[st]
+        layer = (3 - 3 * side, 2 - side, 3 * side, door)[st]
         local(far_in.at[:, pl.ds(pl.multiple_of(layer * strip, strip), strip)], o_send, o_recv.at[st]).wait_recv()
 
     at_door(lambda: ready(1), lambda: ready(0))
-    compute(0)
-    give(0)
-
-    def late_down():
-        pass_on(2, (1, 0), (1, 1))
-        ready(1)
-
-    at_door(lambda: ready(0), late_down)
+    first()
+
+    at_door(lambda: ready(0), lambda: ready(1))
     compute(1)
+    give(1)
+    pass_on(2, (3, 0), (3, 1))
+    merge(0)
     pass_on(2, (2, 0), (2, 1))
-    give(1)
-    give_near(0)
-    give_near(1)
-    merge(0)
-    pass_on(2, (3, 0), (3, 1))
+    ready(3)
+    compute(2)
+    give(2)
+    merge(1)
     ready(2)
-    compute(2)
-    merge(1)
-    give(2)
-    ready(3)
     compute(3)
     give(3)
-    give_near(2)
-    give_near(3)
+    for st in (1, 2, 3):
+        give_near(st)
     merge(2)
     merge(3)
     local(back.at[pl.ds(0, 3 * slots // 2), :], n_send, n_recv.at[0]).wait_recv()
@@ -622,12 +651,12 @@
             pltpu.VMEM((n_fs, depth, hid), bf16), pltpu.VMEM((n_fs, depth, hid), bf16), pltpu.VMEM((n_fs, hid, depth), bf16),
             pltpu.VMEM((count, width), bf16), pltpu.VMEM((3, count, half), bf16), pltpu.VMEM((n_fs, 8, count), f32),
             pltpu.VMEM((4, slots, half), bf16),
-            pltpu.VMEM((n_fs * slots, width), bf16), pltpu.VMEM((n_fs * slots, hid), bf16),
+            pltpu.VMEM((n_fs * slots, width), bf16), pltpu.VMEM((n_fs * slots, hid), f32), pltpu.VMEM((n_fs * slots, hid), bf16),
             pltpu.VMEM((n_fs * slots, width), bf16), pltpu.VMEM((n_fs * slots, half), bf16),
             pltpu.VMEM((n_fs * slots, half), bf16), pltpu.VMEM((quad * slots, half), bf16),
             pltpu.VMEM((2, quad * slots, half), bf16), pltpu.VMEM((2, count, half), bf16), pltpu.VMEM((count, half), bf16),
             pltpu.VMEM((count, quad * slots), bf16), pltpu.VMEM((2, count, quad * slots), bf16),
-            dma((7,)), dma((3,)), dma((3, n_fs - 1)), dma((3,)), dma((2,)), dma((4,)), dma((11,)), dma((3,)), dma((4,)), dma((4,)),
+            dma((7,)), dma((3,)), dma((3, n_fs - 1)), dma((3,)), dma((2,)), dma((4,)), dma((10,)), dma((3,)), dma((4,)), dma((4,)), dma((4,)),
             dma((4, 4)), dma((3,)), dma((4, 2)), dma((4,)),
         ],
         compiler_params=pltpu.CompilerParams(collective_id=2, has_side_effects=True, vmem_limit_bytes=56 * 2**20),

time: 134 us -> 127 us (0.948)
  Pallas kernels: 133 us -> 126 us
    pallas_call x1, Pallas kernels: 130 us -> 123 us  [run_handover(): pl.pallas_call(functools.partial(handover_kernel, sizes), out_shape=[pltp...]
where the time goes in v4:
time: 127 us
  Pallas kernels  126 us (99%)
    pallas_call x1, Pallas kernels, run_handover(): pl.pallas_call(functools.partial(handover_kernel, sizes), out_shape=[pltp...  123 us
    pallas_call x1, Pallas kernels, run_handover(): pl.pallas_call(store_kernel, out_shape=[jax.ShapeDtypeStruct(shape, bf16)...  2.84 us

profile of v4, /device:TPU:0, one launch (start us, length us, event | category | flops | bytes accessed | tf_op | source)
XLA Modules:
  0.0 126.9 jit_solution(3783799859017144429)
XLA Ops:
  0.6 123.4 %handover.1 = (bf16[1,2048,512]{2,1,0:T(8,128)(2,1)S(1)}, bf16[1,2048,512]{2,1,0:T(8,128)(2,1)S(1)}, bf16[1,512,2048]{2,1,0:T(8,128)(2,1)S(1)}, bf16[256,1024]{1,0:T(8,128)(2,1)S(1)}) custom-call(bf16[256,2048]{1,0:T(8,128)(2,1)} %tokens_hbm.1, f32[1,128]{1,0:T(1,128)} %bitcast.5, s32[2,256]{1,0:T(2,128)} %bitcast.3, f32[2,256]{1,0:T(2,128)} %bitcast.4, ...), custom_call_target="tpu_custom_call" | custom-call | tf_op jit(solution)/shard_map/handover/pallas_call | solution.py:643
  124.1 2.8 %store.1 = (bf16[1,2048,512]{2,1,0:T(8,128)(2,1)}, bf16[1,2048,512]{2,1,0:T(8,128)(2,1)}, bf16[1,512,2048]{2,1,0:T(8,128)(2,1)}, bf16[256,1024]{1,0:T(8,128)(2,1)}) custom-call(bf16[1,2048,512]{2,1,0:T(8,128)(2,1)S(1)} %get-tuple-element.8.refs_0_, bf16[1,2048,512]{2,1,0:T(8,128)(2,1)S(1)} %get-tuple-element.9.refs_1_, ...), custom_call_target="tpu_custom_call" | custom-call | tf_op jit(solution)/shard_map/store/pallas_call | solution.py:665

commit v5 on v4

--- a/solution.py
+++ b/solution.py
@@ -226,7 +226,7 @@
 
 def handover_kernel(sizes, tokens_hbm, gain_hbm, ids_hbm, score_hbm, gate_hbm, up_hbm, down_hbm, gate_out, up_out, down_out, mixed,
                     tokens, gain, ids, score, gate_raw, up_raw, down_raw, gate_cut, up_cut, down_cut, rows_own, line_in, meta, y_pick,
-                    picked, gate_act, hidden, part, held, total, back, collect, far_out, far_in, near_w, gate_w,
+                    picked, gate_act, up_act, hidden, part, held, total, back, collect, far_out, far_in, near_w, gate_w,
                     load_sem, w_send, w_recv, g_send, g_recv, d_recv, x_send, x_recv, y_recv, k_recv, t_recv, p_recv, n_recv, c_recv, o_recv):
     n_fs = sizes["fs"]
     g, f, p = lax.axis_index("gr"), lax.axis_index("fs"), lax.axis_index("tp")
@@ -296,7 +296,7 @@
     def g_copy(w, t):
         b = g * n_fs + peer(t)
         src = cuts[w].at[f] if t == (0, 0) else place(w, b)
-        return remote(src, place(w, b), g_send.at[w], g_recv.at[w] if w < 2 else d_recv.at[t[0]], {"gr": 1 - g})
+        return remote(src, place(w, b), g_send.at[w], g_recv.at[0] if w == 0 else d_recv.at[(w - 1) * 4 + t[0]], {"gr": 1 - g})
 
     def pass_on(w, *ts):
         for t in ts:
@@ -304,7 +304,7 @@
             g_copy(w, t).start()
 
     def ready(s):
-        local(down_out.at[0, :, pl.ds(0, strip)], g_send.at[2], d_recv.at[s]).wait_recv()
+        local(down_out.at[0, :, pl.ds(0, strip)], g_send.at[2], d_recv.at[4 + s]).wait_recv()
 
     def row_copy(s):
         if s == 1:
@@ -363,8 +363,21 @@
         y_copy(s).start()
         tp_copy((s, 0)).start()
 
-    def whole(w):
-        local(outs[w].at[0, pl.ds(0, n_fs * depth), :], g_send.at[w], g_recv.at[w]).wait_recv()
+    def whole_gate():
+        local(gate_out.at[0, pl.ds(0, n_fs * depth), :], g_send.at[0], g_recv.at[0]).wait_recv()
+
+    def up_ready(s):
+        local(up_out.at[0, pl.ds(0, strip), :], g_send.at[1], d_recv.at[s]).wait_recv()
+
+    def up_part(s, start, size):
+        k = pl.ds(pl.multiple_of(start, size), size)
+        return jnp.dot(picked[pair(s), k], up_out[0, k, :], preferred_element_type=f32)
+
+    def up_strip(s, layer):
+        return up_part(s, (1 - g) * n_fs * depth + level(layer) * strip, strip)
+
+    def up_of(s):
+        up_act[pair(s), :] = up_part(s, g * n_fs * depth, n_fs * depth) + up_strip(s, 0) + up_strip(s, 1) + up_strip(s, 3)
 
     def gate_of(s):
         blocks = 1 if s == 0 else 2
@@ -464,22 +477,26 @@
         for t in far:
             w_copy(2, t).start()
 
-    whole(0)
+    whole_gate()
     for s in (1, 0, 2):
         gate_of(s)
     at_door(lambda: gate_of(3))
     pass_on(1, (2, 0), (2, 1))
     at_door(early_down)
     far_down()
-    at_end(lambda: take_y(3))
     at_door(lambda: pass_on(2, (1, 0), (1, 1)))
-    whole(1)
-    order = [2, 3, 1, 0]
+    for layer in (0, 1, 3):
+        up_ready(layer)
+    for s in (2, 1, 0):
+        up_of(s)
+    at_door(lambda: up_of(3))
+    up_ready(2)
+    order = [2, 1, 3, 0]
 
     def act(s):
         gated = gate_act[pair(s), :]
-        up_act = jnp.dot(picked[pair(s), :], up_out[0], preferred_element_type=f32)
-        hidden[pair(s), :] = (gated / (1.0 + jnp.exp(-gated)) * up_act).astype(bf16)
+        raised = up_act[pair(s), :] + up_strip(s, 2)
+        hidden[pair(s), :] = (gated / (1.0 + jnp.exp(-gated)) * raised).astype(bf16)
 
     def here(st, base=0):
         layer = (3 * side, door, 3 - 3 * side, 2 - side)[st]
@@ -527,7 +544,11 @@
         for i in range(len(order) + 1):
             if i < len(order):
                 if order[i] == 3:
-                    at_end(lambda: gate_of(3))
+                    def rest():
+                        gate_of(3)
+                        up_of(3)
+
+                    at_end(rest)
                 act(order[i])
             if i:
                 add(0, order[i - 1])
@@ -538,22 +559,25 @@
             if i < len(order):
                 p_copy(0, order[i]).start()
             if i == 0:
+                at_end(lambda: take_y(3))
                 at_end(lambda: pass_on(2, (1, 0), (1, 1)))
         give_near(0)
 
+    later = [3, 2, 1, 0]
+
     def compute(st):
-        for i, s in enumerate(order):
+        for i, s in enumerate(later):
             spread(st, s)
             if i:
-                p_copy(st, order[i - 1]).start()
-        p_copy(st, order[-1]).start()
+                p_copy(st, later[i - 1]).start()
+        p_copy(st, later[-1]).start()
 
     def give(st):
-        for i, s in enumerate(order):
+        for i, s in enumerate(later):
             add(st, s)
             if i:
-                send(st, order[i - 1])
-        send(st, order[-1])
+                send(st, later[i - 1])
+        send(st, later[-1])
 
     def give_near(st):
         n_copy(st, (1, 0)).start()
@@ -561,7 +585,7 @@
 
     def merge(st):
         def act():
-            for i in range(2):
+            for i in (1, 0):
                 local(collect.at[i, pl.ds(0, (quad - 1) * slots), here(st)], c_send, c_recv.at[st, i]).wait_recv()
                 far_out[i, :, here(st)] = jnp.dot(gate_w[i], collect[i, :, here(st)], preferred_element_type=f32).astype(bf16)
                 o_copy(st, i).start()
@@ -578,18 +602,25 @@
     at_door(lambda: ready(0), lambda: ready(1))
     compute(1)
     give(1)
+    at_door(lambda: give_near(1))
     pass_on(2, (3, 0), (3, 1))
     merge(0)
     pass_on(2, (2, 0), (2, 1))
     ready(3)
     compute(2)
     give(2)
+    at_door(lambda: give_near(2))
     merge(1)
     ready(2)
     compute(3)
     give(3)
-    for st in (1, 2, 3):
-        give_near(st)
+    give_near(3)
+
+    def rest_near():
+        give_near(1)
+        give_near(2)
+
+    at_end(rest_near)
     merge(2)
     merge(3)
     local(back.at[pl.ds(0, 3 * slots // 2), :], n_send, n_recv.at[0]).wait_recv()
@@ -651,12 +682,12 @@
             pltpu.VMEM((n_fs, depth, hid), bf16), pltpu.VMEM((n_fs, depth, hid), bf16), pltpu.VMEM((n_fs, hid, depth), bf16),
             pltpu.VMEM((count, width), bf16), pltpu.VMEM((3, count, half), bf16), pltpu.VMEM((n_fs, 8, count), f32),
             pltpu.VMEM((4, slots, half), bf16),
-            pltpu.VMEM((n_fs * slots, width), bf16), pltpu.VMEM((n_fs * slots, hid), f32), pltpu.VMEM((n_fs * slots, hid), bf16),
+            pltpu.VMEM((n_fs * slots, width), bf16), pltpu.VMEM((n_fs * slots, hid), f32), pltpu.VMEM((n_fs * slots, hid), f32), pltpu.VMEM((n_fs * slots, hid), bf16),
             pltpu.VMEM((n_fs * slots, width), bf16), pltpu.VMEM((n_fs * slots, half), bf16),
             pltpu.VMEM((n_fs * slots, half), bf16), pltpu.VMEM((quad * slots, half), bf16),
             pltpu.VMEM((2, quad * slots, half), bf16), pltpu.VMEM((2, count, half), bf16), pltpu.VMEM((count, half), bf16),
             pltpu.VMEM((count, quad * slots), bf16), pltpu.VMEM((2, count, quad * slots), bf16),
-            dma((7,)), dma((3,)), dma((3, n_fs - 1)), dma((3,)), dma((2,)), dma((4,)), dma((10,)), dma((3,)), dma((4,)), dma((4,)), dma((4,)),
+            dma((7,)), dma((3,)), dma((3, n_fs - 1)), dma((3,)), dma((1,)), dma((8,)), dma((10,)), dma((3,)), dma((4,)), dma((4,)), dma((4,)),
             dma((4, 4)), dma((3,)), dma((4, 2)), dma((4,)),
         ],
         compiler_params=pltpu.CompilerParams(collective_id=2, has_side_effects=True, vmem_limit_bytes=56 * 2**20),

time: 127 us -> 127 us (level); the launches traced: 127 us -> 125 us
  Pallas kernels: 126 us -> 124 us
    pallas_call x1, Pallas kernels: 123 us -> 122 us  [run_handover(): pl.pallas_call(functools.partial(handover_kernel, sizes), out_shape=[pltp...]
where the time goes in v5:
time: 127 us; the launch traced here: 125 us
  Pallas kernels  124 us (98%)
    pallas_call x1, Pallas kernels, run_handover(): pl.pallas_call(functools.partial(handover_kernel, sizes), out_shape=[pltp...  122 us
    pallas_call x1, Pallas kernels, run_handover(): pl.pallas_call(store_kernel, out_shape=[jax.ShapeDtypeStruct(shape, bf16)...  2.84 us

profile of v5, /device:TPU:0, one launch (start us, length us, event | category | flops | bytes accessed | tf_op | source)
XLA Modules:
  0.0 125.1 jit_solution(11697133308821767417)
XLA Ops:
  0.6 121.6 %handover.1 = (bf16[1,2048,512]{2,1,0:T(8,128)(2,1)S(1)}, bf16[1,2048,512]{2,1,0:T(8,128)(2,1)S(1)}, bf16[1,512,2048]{2,1,0:T(8,128)(2,1)S(1)}, bf16[256,1024]{1,0:T(8,128)(2,1)S(1)}) custom-call(bf16[256,2048]{1,0:T(8,128)(2,1)} %tokens_hbm.1, f32[1,128]{1,0:T(1,128)} %bitcast.5, s32[2,256]{1,0:T(2,128)} %bitcast.3, f32[2,256]{1,0:T(2,128)} %bitcast.4, ...), custom_call_target="tpu_custom_call" | custom-call | tf_op jit(solution)/shard_map/handover/pallas_call | solution.py:674
  122.2 2.8 %store.1 = (bf16[1,2048,512]{2,1,0:T(8,128)(2,1)}, bf16[1,2048,512]{2,1,0:T(8,128)(2,1)}, bf16[1,512,2048]{2,1,0:T(8,128)(2,1)}, bf16[256,1024]{1,0:T(8,128)(2,1)}) custom-call(bf16[1,2048,512]{2,1,0:T(8,128)(2,1)S(1)} %get-tuple-element.8.refs_0_, bf16[1,2048,512]{2,1,0:T(8,128)(2,1)S(1)} %get-tuple-element.9.refs_1_, ...), custom_call_target="tpu_custom_call" | custom-call | tf_op jit(solution)/shard_map/store/pallas_call | solution.py:696

commit v6 on v5

--- a/solution.py
+++ b/solution.py
@@ -602,7 +602,7 @@
     at_door(lambda: ready(0), lambda: ready(1))
     compute(1)
     give(1)
-    at_door(lambda: give_near(1))
+    give_near(1)
     pass_on(2, (3, 0), (3, 1))
     merge(0)
     pass_on(2, (2, 0), (2, 1))
@@ -616,11 +616,7 @@
     give(3)
     give_near(3)
 
-    def rest_near():
-        give_near(1)
-        give_near(2)
-
-    at_end(rest_near)
+    at_end(lambda: give_near(2))
     merge(2)
     merge(3)
     local(back.at[pl.ds(0, 3 * slots // 2), :], n_send, n_recv.at[0]).wait_recv()

time: 127 us -> 126 us (level); the launches traced: 125 us -> 126 us
  no operation moved by 1% of the time
where the time goes in v6:
time: 126 us
  Pallas kernels  125 us (99%)
    pallas_call x1, Pallas kernels, run_handover(): pl.pallas_call(functools.partial(handover_kernel, sizes), out_shape=[pltp...  123 us
    pallas_call x1, Pallas kernels, run_handover(): pl.pallas_call(store_kernel, out_shape=[jax.ShapeDtypeStruct(shape, bf16)...  2.84 us

profile of v6, /device:TPU:0, one launch (start us, length us, event | category | flops | bytes accessed | tf_op | source)
XLA Modules:
  0.0 126.0 jit_solution(14719957272451374506)
XLA Ops:
  0.6 122.6 %handover.1 = (bf16[1,2048,512]{2,1,0:T(8,128)(2,1)S(1)}, bf16[1,2048,512]{2,1,0:T(8,128)(2,1)S(1)}, bf16[1,512,2048]{2,1,0:T(8,128)(2,1)S(1)}, bf16[256,1024]{1,0:T(8,128)(2,1)S(1)}) custom-call(bf16[256,2048]{1,0:T(8,128)(2,1)} %tokens_hbm.1, f32[1,128]{1,0:T(1,128)} %bitcast.5, s32[2,256]{1,0:T(2,128)} %bitcast.3, f32[2,256]{1,0:T(2,128)} %bitcast.4, ...), custom_call_target="tpu_custom_call" | custom-call | tf_op jit(solution)/shard_map/handover/pallas_call | solution.py:670
  123.2 2.8 %store.1 = (bf16[1,2048,512]{2,1,0:T(8,128)(2,1)}, bf16[1,2048,512]{2,1,0:T(8,128)(2,1)}, bf16[1,512,2048]{2,1,0:T(8,128)(2,1)}, bf16[256,1024]{1,0:T(8,128)(2,1)}) custom-call(bf16[1,2048,512]{2,1,0:T(8,128)(2,1)S(1)} %get-tuple-element.8.refs_0_, bf16[1,2048,512]{2,1,0:T(8,128)(2,1)S(1)} %get-tuple-element.9.refs_1_, ...), custom_call_target="tpu_custom_call" | custom-call | tf_op jit(solution)/shard_map/store/pallas_call | solution.py:692
